TPU v7x, 512 devices: a whole 4x4x16 slice. The times are simulated.
512 devices in a mesh: ep: 32 (over z, core), tp: 16 (over y, x).
Axes of the slice: x: 4, y: 4, z: 16, core: 2. Of those that a mesh axis runs over, the one named last changes fastest.
Arguments:
- query_rows: bfloat16 [24576, 1024], P('ep', 'tp'), may hold values from -600 to 600
- key_rows: bfloat16 [24576, 1024], P('ep', 'tp'), may hold values from -6 to 6
- value_rows: bfloat16 [24576, 1024], P('ep', 'tp'), may hold values from -6 to 6
- cum_gate: float32 [16, 24576], P('tp'), may hold values from -2458 to 0, as said below
- out_weight: bfloat16 [1024, 2048], P(None, 'tp'), may hold values from -0.1875 to 0.1875
- moe_input: bfloat16 [6144, 2048], P('ep'), may hold values from -6 to 6
- moe_gain: float32 [2048], replicated, may hold values from 0.1 to 1.9
- routes: int32 [6144, 3], P('ep'), may hold values from 0 to 127, all different within a row; in each aligned block of 192 rows (0 to 191, 192 to 383, ...) at most 9 rows name the same one
- route_weight: float32 [6144, 3], P('ep'), may hold values from 0.2 to 1.5
- expert_gate: bfloat16 [128, 2048, 512], P('ep', None, 'tp'), may hold values from -0.125 to 0.125
- expert_up: bfloat16 [128, 2048, 512], P('ep', None, 'tp'), may hold values from -0.125 to 0.125
- expert_down: bfloat16 [128, 512, 2048], P('ep', None, 'tp'), may hold values from -0.25 to 0.25
- shared_gate: bfloat16 [2048, 512], P(None, 'tp'), may hold values from -0.125 to 0.125
- shared_up: bfloat16 [2048, 512], P(None, 'tp'), may hold values from -0.125 to 0.125
- shared_down: bfloat16 [512, 2048], P(None, 'tp'), may hold values from -0.25 to 0.25
Outputs:
- mixer_out: bfloat16 [24576, 2048], P('ep', 'tp')
- moe_out: bfloat16 [6144, 2048], P('ep', 'tp')
Inputs may be any that keep to these rules, and one draw needn't show every extreme that they name: Non-increasing along positions: cum_gate[h, t] is the sum of the log forget gates of head h over positions 0 to t. `routes`: the 3 experts of a token differ. In each aligned block of 192 tokens no expert is named by more than 9 tokens, a bound that some block reaches.
All inputs are finite; a program needn't handle non-finite values.
Results may differ from a plain program's by a relative error of at most 0.0068.
Values may be sent and summed in bfloat16 or wider, within the bound.
No kernel may reach another device: no remote copies, remote signals or barrier semaphores. Data moves between devices by JAX's collectives and lax.ppermute only.
A program may use at most 64 MiB of HBM per device.

v0:
```python
import jax
import jax.numpy as jnp
from jax import lax
from jax.sharding import PartitionSpec as P

HEAD = 64


neg_fill = -1e30
norm_eps = 1e-06


def joined_along(pieces, dim):
    dims = list(pieces.shape[1:])
    dims[dim] *= pieces.shape[0]
    return jnp.moveaxis(pieces, 0, dim).reshape(dims)


def sent_to_all(array, axis):
    copies = jnp.broadcast_to(array, (lax.axis_size(axis), *array.shape))
    return lax.all_to_all(copies, axis, split_axis=0, concat_axis=0, tiled=True)


def collect(array, axis, dim):
    return joined_along(sent_to_all(array, axis), dim)


def local(
    query_rows,
    key_rows,
    value_rows,
    cum_gate,
    out_weight,
    moe_input,
    moe_gain,
    routes,
    route_weight,
    expert_gate,
    expert_up,
    expert_down,
    shared_gate,
    shared_up,
    shared_down,
):
    row_count = query_rows.shape[0]
    width = query_rows.shape[1]
    local_heads = width // HEAD
    scale = HEAD ** (-0.5)
    first_row = lax.axis_index("ep") * row_count
    last_row = first_row + row_count - 1
    query_heads = query_rows.reshape(row_count, local_heads, HEAD)
    query_gate = lax.dynamic_slice_in_dim(cum_gate, first_row, row_count, 1)
    query_pos = first_row + jnp.arange(row_count, dtype=jnp.int32)
    key_value = jnp.concatenate([key_rows, value_rows], axis=1)
    initial = (
        jnp.full((local_heads, row_count), neg_fill, jnp.float32),
        jnp.zeros((local_heads, row_count), jnp.float32),
        jnp.zeros((local_heads, row_count, HEAD), jnp.float32),
    )
    shard_rows = lax.all_gather(key_value, "ep", axis=0, tiled=True)
    piece_len = shard_rows.shape[0]
    key_span = 512

    def one_span(state_in, span_index):
        span_start = span_index * key_span

        def update(state_old):
            running_max, denominator, weighted = state_old
            block = lax.dynamic_slice_in_dim(shard_rows, span_index * key_span, key_span, 0)
            keys_block = block[:, :width].reshape(key_span, local_heads, HEAD)
            values_block = block[:, width:].reshape(key_span, local_heads, HEAD)
            key_gate = lax.dynamic_slice_in_dim(cum_gate, span_start, key_span, 1)
            scores = (
                jnp.einsum(
                    "qhd,khd->hqk", query_heads, keys_block, preferred_element_type=jnp.float32
                )
                * scale
            )
            scores = scores + query_gate[:, :, None] - key_gate[:, None, :]
            causal = (span_start + jnp.arange(key_span, dtype=jnp.int32))[None, :] <= query_pos[
                :, None
            ]
            scores = jnp.where(causal[None], scores, neg_fill)
            new_max = jnp.maximum(running_max, jnp.max(scores, axis=2))
            expon = jnp.where(causal[None], jnp.exp(scores - new_max[:, :, None]), 0.0)
            rescale = jnp.exp(running_max - new_max)
            denominator = denominator * rescale + jnp.sum(expon, axis=2)
            weighted = weighted * rescale[:, :, None] + jnp.einsum(
                "hqk,khd->hqd",
                expon.astype(jnp.bfloat16),
                values_block,
                preferred_element_type=jnp.float32,
            )
            return (new_max, denominator, weighted)

        state_next = lax.cond(span_start <= last_row, update, lambda unchanged: unchanged, state_in)
        return (state_next, None)

    state_out, _ = lax.scan(one_span, initial, jnp.arange(piece_len // key_span, dtype=jnp.int32))
    running_max, denominator, weighted = state_out
    heads_out = (weighted / denominator[:, :, None]).transpose(1, 0, 2).reshape(row_count, width)
    heads_out = heads_out.astype(jnp.bfloat16)
    token_count = moe_input.shape[0]
    top_count = routes.shape[1]
    local_experts = expert_gate.shape[0]
    ep_count = lax.axis_size("ep")
    expert_count = local_experts * ep_count
    capacity = 2 * token_count * top_count // expert_count
    column_count = expert_down.shape[2]
    first_column = lax.axis_index("tp") * column_count
    moe_rows = moe_input.astype(jnp.float32)
    normed = (
        moe_rows
        * lax.rsqrt(jnp.mean(moe_rows * moe_rows, axis=1, keepdims=True) + norm_eps)
        * moe_gain
    ).astype(jnp.bfloat16)
    flat_routes = routes.reshape(-1)
    one_hot = (flat_routes[:, None] == jnp.arange(expert_count, dtype=jnp.int32)[None, :]).astype(
        jnp.int32
    )
    ranks = jnp.sum(jnp.cumsum(one_hot, axis=0) * one_hot, axis=1) - 1
    slot_index = flat_routes * capacity + ranks
    pair_token = jnp.arange(token_count * top_count, dtype=jnp.int32) // top_count
    slot_token = (
        jnp.full((expert_count * capacity,), token_count, jnp.int32).at[slot_index].set(pair_token)
    )
    padded = jnp.concatenate([normed, jnp.zeros((1, normed.shape[1]), jnp.bfloat16)], axis=0)
    outgoing = lax.dynamic_slice_in_dim(padded, first_column, column_count, 1)[slot_token]
    outgoing = outgoing.reshape(ep_count, local_experts, capacity, outgoing.shape[1])
    arrived = lax.all_to_all(outgoing, "ep", split_axis=0, concat_axis=0, tiled=True)
    arrived = lax.all_gather(arrived, "tp", axis=3, tiled=True)
    gate_val = jnp.einsum(
        "aecd,edf->aecf", arrived, expert_gate, preferred_element_type=jnp.float32
    )
    up_val = jnp.einsum("aecd,edf->aecf", arrived, expert_up, preferred_element_type=jnp.float32)
    hidden = (jax.nn.silu(gate_val) * up_val).astype(jnp.bfloat16)
    hidden = collect(hidden, "tp", 3)
    result = jnp.einsum(
        "aecf,efd->aecd", hidden, expert_down, preferred_element_type=jnp.float32
    ).astype(jnp.bfloat16)
    returned = lax.all_to_all(result, "ep", split_axis=0, concat_axis=0, tiled=True)
    picked = returned.reshape(expert_count * capacity, column_count)[slot_index]
    picked = picked.astype(jnp.float32).reshape(token_count, top_count, column_count)
    routed = jnp.sum(picked * route_weight[:, :, None], axis=1)
    shared_hidden = (
        jax.nn.silu(jnp.dot(normed, shared_gate, preferred_element_type=jnp.float32))
        * jnp.dot(normed, shared_up, preferred_element_type=jnp.float32)
    ).astype(jnp.bfloat16)
    mixer_sum = jnp.dot(
        lax.all_gather(heads_out, "tp", axis=1, tiled=True),
        out_weight,
        preferred_element_type=jnp.float32,
    )
    shared_all = lax.all_gather(shared_hidden, "tp", axis=1, tiled=True)
    moe_total = routed + jnp.dot(shared_all, shared_down, preferred_element_type=jnp.float32)
    return (mixer_sum.astype(jnp.bfloat16), moe_total.astype(jnp.bfloat16))


def solution(mesh):
    placed = (
        P("ep", "tp"),
        P("ep", "tp"),
        P("ep", "tp"),
        P("tp", None),
        P(None, "tp"),
        P("ep", None),
        P(),
        P("ep", None),
        P("ep", None),
        P("ep", None, "tp"),
        P("ep", None, "tp"),
        P("ep", None, "tp"),
        P(None, "tp"),
        P(None, "tp"),
        P(None, "tp"),
    )
    return jax.shard_map(
        local, mesh=mesh, in_specs=placed, out_specs=(P("ep", "tp"), P("ep", "tp")), check_vma=False
    )
```

profile of v0, /device:TPU:1, one launch (start us, length us, event | category | flops | bytes accessed | tf_op | source)
XLA Modules:
  0.0 554.8 jit_solution(1330439696241112962)
XLA Ops:
  11.6 4.1 scatter_custom_fusion
  16.0 2.9 gather_fusion
  19.3 40.2 %all_to_all.15 = bf16[32,4,9,128]{3,1,2,0:T(4,128)(2,1)S(1)} all-to-all(bf16[32,4,9,128]{3,1,2,0:T(4,128)(2,1)S(1)} %copy.46), channel_id=1, replica_groups=mesh['ep'=32,'tp'=16] {'ep'}, dimensions={0} | all-to-all | bytes 589824 | tf_op jit(solution)/shard_map/all_to_all | solution.py:130
  61.6 63.6 %all-gather.7.cloned.1.call-done = bf16[32,4,9,2048]{3,0,2,1:T(8,128)(2,1)} async-done(((bf16[32,4,9,128]{3,0,2,1:T(8,128)(2,1)}), bf16[32,4,9,2048]{3,0,2,1:T(8,128)(2,1)}) %all-gather.7.cloned.1.call-update) | async-done | bytes 4718608 | tf_op jit(solution)/shard_map/all_gather | solution.py:131
  125.2 3.8 convolution_bitcast_fusion.2
  130.5 3.2 broadcast_bitcast_fusion
  133.7 7.8 %reshape.164 = bf16[16,2,18432]{2,1,0:T(2,128)(2,1)} reshape(bf16[16,4,9,32,32]{4,3,2,1,0:T(8,128)(2,1)} %broadcast_bitcast_fusion) | data formatting | bytes 2359296
  141.5 4.8 all-to-all-start.1
  147.2 58.1 %all-gather.5.cloned.1.call-done = bf16[24576,128]{1,0:T(8,128)(2,1)} async-done(((bf16[768,128]{1,0:T(8,128)(2,1)}), bf16[24576,128]{1,0:T(8,128)(2,1)}) %all-gather.5.cloned.1.call-update) | async-done | bytes 6291472 | tf_op jit(solution)/shard_map/all_gather | solution.py:60
  205.4 76.2 %while.15 = (s32[]{:T(128)}, f32[1,768]{1,0:T(1,128)S(1)}, f32[1,768]{1,0:T(1,128)S(1)}, f32[1,768,64]{1,2,0:T(8,128)S(1)}, s32[48]{0:T(128)S(1)}, /*index=5*/s3...) while((s32[]{:T(128)}, f32[1,768]{1,0:T(1,128)S(1)}, ...), condition=%wide.region_5.6_spmd.clone, body=%wide.region_0.5_spmd.clone.sunk | while | flops 106270224 | bytes 5566899 | solution.py:99
  206.7 4.7 conditional.3
  209.6 1.4 fusion.4
  212.6 4.7 conditional.3
  215.5 1.4 fusion.4
  218.6 4.7 conditional.3
  282.3 3.8 reshape.165
  286.1 3.1 bitcast_bitcast_fusion
  289.2 7.6 %copy.48 = bf16[32,4,9,16,32]{4,3,0,2,1:T(8,128)(2,1)} copy(bf16[32,4,9,16,32]{4,0,2,1,3:T(8,128)(2,1)S(1)} %bitcast_bitcast_fusion) | data formatting | bytes 2359296 | tf_op jit(solution)/shard_map/transpose | solution.py:16
  296.8 6.5 %reshape.124 = bf16[32,4,9,512]{3,0,2,1:T(8,128)(2,1)S(1)} reshape(bf16[32,4,9,16,32]{4,3,0,2,1:T(8,128)(2,1)} %copy.48) | data formatting | bytes 2359296 | tf_op jit(solution)/shard_map/reshape | solution.py:16
  304.7 213.7 %all-to-all-start.2 = ((bf16[32,4,9,128]{3,1,2,0:T(4,128)(2,1)}), bf16[32,4,9,128]{3,1,2,0:T(4,128)(2,1)S(1)}, u32[]{:S(2)}, u32[]{:S(2)}) async-start(bf16[32,4,9,128]{3,1,2,0:T(4,128)(2,1)} %copy.49), calls=%async_computation.2 | async-start | bytes 589824 | tf_op jit(solution)/shard_map/all_to_all | solution.py:141
  519.2 20.5 %all_gather.15 = bf16[192,512]{0,1:T(8,128)(2,1)S(1)} all-gather(bf16[192,32]{0,1:T(8,128)(2,1)S(1)} %fusion.27), channel_id=1, replica_groups=mesh['ep'=32,'tp'=16] {'tp'}, dimensions={1}, use_global_device_ids=true | all-gather | bytes 208896 | tf_op jit(solution)/shard_map/all_gather | solution.py:154
  539.7 2.2 all-to-all-done.2
  542.2 1.9 gather_fusion.1
  545.5 2.7 fusion.22
  (252 shorter events, 51.7 us)
Async XLA Ops:
  7.2 296.1 %copy-start = (bf16[4,512,128]{2,1,0:T(8,128)(2,1)S(1)}, bf16[4,512,128]{2,1,0:T(8,128)(2,1)}, u32[]{:S(2)}) copy-start(bf16[4,512,128]{2,1,0:T(8,128)(2,1)} %param.30) | copy-start | bytes 1572868
  7.2 118.0 %all-gather.7.cloned.1.call-start = ((), (), s32[]{:S(2)}) async-start(), calls=%async_computation.4 | async-start | bytes 5013504 | tf_op jit(solution)/shard_map/all_gather | solution.py:131
  10.9 4.8 copy-start.1
  10.9 4.8 copy-start.8
  19.0 41.4 %copy-start.6 = (bf16[768,64]{0,1:T(8,128)(2,1)S(1)}, bf16[768,64]{0,1:T(8,128)(2,1)}, u32[]{:S(2)}) copy-start(bf16[768,64]{0,1:T(8,128)(2,1)} %param.20) | copy-start | bytes 294916
  19.0 41.6 %copy-start.7 = (bf16[768,64]{0,1:T(8,128)(2,1)S(1)}, bf16[768,64]{0,1:T(8,128)(2,1)}, u32[]{:S(2)}) copy-start(bf16[768,64]{0,1:T(8,128)(2,1)} %param.21) | copy-start | bytes 294916
  19.3 105.9 %copy-start.11 = (bf16[4,2048,32]{1,2,0:T(8,128)(2,1)S(1)}, bf16[4,2048,32]{1,2,0:T(8,128)(2,1)}, u32[]{:S(2)}) copy-start(bf16[4,2048,32]{1,2,0:T(8,128)(2,1)} %param.28) | copy-start | bytes 1572868
  60.3 145.0 %all-gather.5.cloned.1.call-start = ((), (), s32[]{:S(2)}) async-start(), calls=%async_computation.3 | async-start | bytes 6488064 | tf_op jit(solution)/shard_map/all_gather | solution.py:60
  61.6 67.5 %copy-start.12 = (bf16[4,2048,32]{1,2,0:T(8,128)(2,1)S(1)}, bf16[4,2048,32]{1,2,0:T(8,128)(2,1)}, u32[]{:S(2)}) copy-start(bf16[4,2048,32]{1,2,0:T(8,128)(2,1)} %param.29) | copy-start | bytes 1572868
  125.2 3.9 copy-start.10
  141.5 63.9 %copy-start.13 = (bf16[768,64]{0,1:T(8,128)(2,1)S(1)}, bf16[768,64]{0,1:T(8,128)(2,1)}, u32[]{:S(2)}) copy-start(bf16[768,64]{0,1:T(8,128)(2,1)} %param.19) | copy-start | bytes 294916
  141.5 140.8 %all-to-all-start.1 = ((bf16[16,2,18432]{2,1,0:T(2,128)(2,1)}), bf16[16,2,18432]{2,1,0:T(2,128)(2,1)S(1)}, u32[]{:S(2)}, u32[]{:S(2)}) async-start(bf16[16,2,18432]{2,1,0:T(2,128)(2,1)} %reshape.164), calls=%async_computation.1 | async-start | bytes 2359296 | tf_op jit(solution)/shard_map/all_to_all | solution.py:21
  146.3 399.2 %all-gather.9.cloned.1.call-start = ((), (), s32[]{:S(2)}) async-start(), calls=%async_computation.5 | async-start | bytes 1671168 | tf_op jit(solution)/shard_map/all_gather | solution.py:150
  303.3 215.1 %copy-start.9 = (f32[192,3]{0,1:T(4,128)S(1)}, f32[192,3]{0,1:T(4,128)}, u32[]{:S(2)}) copy-start(f32[192,3]{0,1:T(4,128)} %param.27) | copy-start | bytes 6916
  303.3 215.2 %copy-start.4 = (bf16[2048,32]{0,1:T(8,128)(2,1)S(1)}, bf16[2048,32]{0,1:T(8,128)(2,1)}, u32[]{:S(2)}) copy-start(bf16[2048,32]{0,1:T(8,128)(2,1)} %param.31) | copy-start | bytes 393220
  303.8 215.1 %copy-start.5 = (bf16[2048,32]{0,1:T(8,128)(2,1)S(1)}, bf16[2048,32]{0,1:T(8,128)(2,1)}, u32[]{:S(2)}) copy-start(bf16[2048,32]{0,1:T(8,128)(2,1)} %param.32) | copy-start | bytes 393220
  304.7 237.3 %all-to-all-start.2 = ((bf16[32,4,9,128]{3,1,2,0:T(4,128)(2,1)}), bf16[32,4,9,128]{3,1,2,0:T(4,128)(2,1)S(1)}, u32[]{:S(2)}, u32[]{:S(2)}) async-start(bf16[32,4,9,128]{3,1,2,0:T(4,128)(2,1)} %copy.49), calls=%async_computation.2 | async-start | bytes 589824 | tf_op jit(solution)/shard_map/all_to_all | solution.py:141
  542.1 2.6 copy-start.3
  542.2 3.3 copy-start.2
Sparse Core Ops, SparseCore 0:
  60.4 64.7 all-gather.6
  127.9 77.4 all-gather.4
  282.4 260.1 all-gather.8
where the time goes:
time: 559 us; the launch traced here: 555 us
  starting transfers between devices  219 us (39%)
  waiting for transfers between devices  124 us (22%)
  local copies, waits for them, and re-layouts  76.5 us (14%)
  blocking collectives  60.7 us (11%)
  loops' own time  36.1 us (6%)
  matrix products  18.3 us (3%)
  between operations  14.2 us (3%)
  other arithmetic  6.13 us (1%)
    all_to_all x1, starting transfers between devices, local(): lax.all_to_all(result, 'ep', split_axis=0, concat_axis=0, tiled=True)  214 us
    all_gather x1, waiting for transfers between devices, local(): arrived = lax.all_gather(arrived, 'tp', axis=3, tiled=True)  63.6 us
    all_gather x1, waiting for transfers between devices, local(): shard_rows = lax.all_gather(key_value, 'ep', axis=0, tiled=True)  58.1 us
    all_to_all x1, blocking collectives, local(): lax.all_to_all(outgoing, 'ep', split_axis=0, concat_axis=0, tiled=True)  40.2 us
    another operation x1, loops' own time, local(): lax.scan(one_span, initial, jnp.arange(piece_len // key_span, dtype=jnp.i...  33.2 us
    dynamic_slice x48, local copies, waits for them, and re-layouts, local(): lax.scan(one_span, initial, jnp.arange(piece_len // key_span, dtype=jnp.i...  28.1 us
    all_gather x1, blocking collectives, local(): shared_all = lax.all_gather(shared_hidden, 'tp', axis=1, tiled=True)  20.5 us
    unnamed x35, local copies, waits for them, and re-layouts  16.1 us
  transfers between devices with their start and end apart: 5, of which 3 were waited for; matrix products, arithmetic and copies ran while one was open for 15% of the time, Pallas kernels for 0%

commit v1 on v0

v1 whole, which is shorter than its diff:
```python
import functools

import jax
import jax.numpy as jnp
from jax import lax
from jax.experimental import pallas as pl
from jax.experimental.pallas import tpu as pltpu
from jax.sharding import PartitionSpec as P

HEAD = 64
CAP = 9
LOG2E = 1.4426950408889634
neg_fill = -1e30
norm_eps = 1e-06
F32 = jnp.float32
BF16 = jnp.bfloat16
NT = (((1,), (1,)), ((), ()))
TN = (((0,), (0,)), ((), ()))
NN = (((1,), (0,)), ((), ()))


def dot(a, b, dims=NN):
    return lax.dot_general(a, b, dims, preferred_element_type=F32)


def sent_to_all(array, axis):
    copies = jnp.broadcast_to(array, (lax.axis_size(axis), *array.shape))
    return lax.all_to_all(copies, axis, split_axis=0, concat_axis=0, tiled=True)


def cost(flops, nbytes):
    return pl.CostEstimate(flops=flops, transcendentals=0, bytes_accessed=nbytes)


def attention_kernel(ep_ref, q_ref, kv_ref, gk_ref, g0_ref, out_ref, q_scr, m_scr, acc_scr, *, tile):
    step = pl.program_id(0)
    own = ep_ref[0]
    rows = q_scr.shape[0]
    keys = kv_ref.shape[2]

    @pl.when(step == 0)
    def _():
        q_scr[...] = q_ref[...].T
        m_scr[...] = jnp.full(m_scr.shape, neg_fill, F32)
        acc_scr[...] = jnp.zeros(acc_scr.shape, F32)

    def update(diagonal):
        kt = kv_ref[0, :HEAD, :]
        row_id = lax.broadcasted_iota(jnp.int32, (2 * HEAD, keys), 0)
        vt = jnp.where(row_id < HEAD, jnp.ones((), BF16), kv_ref[0].astype(BF16))
        gate = (gk_ref[...] - g0_ref[:, :1]) * LOG2E
        for i in range(rows // tile):
            span = pl.ds(i * tile, tile)
            used = min(keys, (i + 1) * tile) if diagonal else keys
            s = dot(q_scr[span, :], kt[:, :used]) * (LOG2E * HEAD**-0.5) - gate[:, :used]
            if diagonal:
                q_pos = i * tile + lax.broadcasted_iota(jnp.int32, (tile, used), 0)
                k_pos = lax.broadcasted_iota(jnp.int32, (tile, used), 1)
                s = jnp.where(k_pos <= q_pos, s, neg_fill)
            old = m_scr[span, :1]
            new = jnp.maximum(old, jnp.max(s, axis=1, keepdims=True))
            p = jnp.exp2(s - new).astype(BF16)
            acc_scr[span, :] = acc_scr[span, :] * jnp.exp2(old - new) + dot(p, vt[:, :used], NT)
            m_scr[span, :] = jnp.broadcast_to(new, (tile, m_scr.shape[1]))

    @pl.when(step == 0)
    def _():
        update(True)

    @pl.when((step > 0) & (step <= own))
    def _():
        update(False)

    @pl.when(step == pl.num_programs(0) - 1)
    def _():
        half = rows // 2
        top = acc_scr[:half, :]
        low = acc_scr[half:, :]
        out_ref[...] = jnp.concatenate(
            [top[:, HEAD:] / top[:, :HEAD], low[:, HEAD:] / low[:, :HEAD]], axis=1
        ).astype(BF16)


def attention(ep_index, q_t, kv_all, cum_gate):
    blocks, wide, keys = kv_all.shape
    rows = q_t.shape[1]

    def place(j, ep):
        return jnp.where(j == 0, ep[0], jnp.maximum(jnp.minimum(j, ep[0]) - 1, 0))

    return pl.pallas_call(
        functools.partial(attention_kernel, tile=256),
        grid_spec=pltpu.PrefetchScalarGridSpec(
            num_scalar_prefetch=1,
            grid=(blocks,),
            in_specs=[
                pl.BlockSpec((HEAD, rows), lambda j, ep: (0, 0)),
                pl.BlockSpec((1, wide, keys), lambda j, ep: (place(j, ep), 0, 0)),
                pl.BlockSpec((1, keys), lambda j, ep: (0, place(j, ep))),
                pl.BlockSpec((1, keys), lambda j, ep: (0, ep[0])),
            ],
            out_specs=pl.BlockSpec((rows // 2, 2 * HEAD), lambda j, ep: (0, 0)),
            scratch_shapes=[
                pltpu.VMEM((rows, HEAD), BF16),
                pltpu.VMEM((rows, 128), F32),
                pltpu.VMEM((rows, 128), F32),
            ],
        ),
        out_shape=jax.ShapeDtypeStruct((rows // 2, 2 * HEAD), BF16),
        compiler_params=pltpu.CompilerParams(dimension_semantics=("arbitrary",)),
        cost_estimate=cost(2 * 2 * rows * keys * blocks * 256, 8 << 20),
        name="attention",
    )(ep_index, q_t, kv_all, cum_gate, cum_gate)


def projection_kernel(heads_ref, w_ref, out_ref):
    count, half, _ = heads_ref.shape
    acc = jnp.zeros((half, 2 * w_ref.shape[1]), F32)
    blank = jnp.zeros((HEAD, w_ref.shape[1]), BF16)
    for h in range(count):
        w = w_ref[h * HEAD : (h + 1) * HEAD, :]
        both = jnp.concatenate(
            [jnp.concatenate([w, blank], axis=1), jnp.concatenate([blank, w], axis=1)], axis=0
        )
        acc = acc + dot(heads_ref[h], both)
    out_ref[:half, :] = acc[:, : w_ref.shape[1]].astype(BF16)
    out_ref[half:, :] = acc[:, w_ref.shape[1] :].astype(BF16)


def projection(heads, out_weight):
    count, half, _ = heads.shape
    columns = out_weight.shape[1]
    return pl.pallas_call(
        projection_kernel,
        out_shape=jax.ShapeDtypeStruct((2 * half, columns), BF16),
        cost_estimate=cost(2 * half * count * 128 * 256, 4 << 20),
        name="projection",
    )(heads, out_weight)


def spread_kernel(gate_ref, up_ref, out_ref):
    peers = out_ref.shape[0]
    for t in range(peers):
        out_ref[t, 0] = gate_ref[:, :, t * 128 : (t + 1) * 128]
        out_ref[t, 1] = up_ref[:, :, t * 128 : (t + 1) * 128]


def spread_weights(gate_t, up_t, peers):
    experts, hidden, width = gate_t.shape
    return pl.pallas_call(
        spread_kernel,
        out_shape=jax.ShapeDtypeStruct((peers, 2, experts, hidden, width // peers), BF16),
        name="spread",
    )(gate_t, up_t)


def route_kernel(
    tp_ref, x_ref, gain_ref, routes_ref, weight_ref, sg_ref, su_ref, slot_ref, mix_ref, shared_ref, norm_scr,
    *, groups, local_experts, room,
):
    tokens = x_ref.shape[0]
    x = x_ref[...].astype(F32)
    scale = lax.rsqrt(jnp.mean(x * x, axis=1, keepdims=True) + norm_eps)
    normed = (x * scale * gain_ref[...]).astype(BF16)
    norm_scr[...] = normed
    columns = slot_ref.shape[1]
    piece = norm_scr[:, pl.ds(pl.multiple_of(tp_ref[0] * columns, columns), columns)]
    slots = groups * room
    shape = (groups, room, tokens)
    within = lax.broadcasted_iota(jnp.int32, shape, 1)
    expert = lax.broadcasted_iota(jnp.int32, shape, 0) * local_experts + within % local_experts
    expert = expert.reshape(slots, tokens)
    turn = (within // local_experts).reshape(slots, tokens).astype(F32)
    hit = jnp.zeros((slots, tokens), F32)
    weight = jnp.zeros((slots, tokens), F32)
    for j in range(routes_ref.shape[0]):
        same = expert == routes_ref[j : j + 1, :]
        hit = hit + jnp.where(same, 1.0, 0.0)
        weight = weight + jnp.where(same, weight_ref[j : j + 1, :], 0.0)
    before = lax.broadcasted_iota(jnp.int32, (tokens, tokens), 0)
    after = lax.broadcasted_iota(jnp.int32, (tokens, tokens), 1)
    earlier = jnp.where(before < after, 1.0, 0.0).astype(BF16)
    rank = dot(hit.astype(BF16), earlier)
    chosen = jnp.where(rank == turn, hit, 0.0)
    slot_ref[...] = dot(chosen.astype(BF16), piece).astype(BF16)
    mix = chosen * weight
    coarse = mix.astype(BF16)
    mix_ref[0] = coarse
    mix_ref[1] = (mix - coarse.astype(F32)).astype(BF16)
    gate_val = dot(sg_ref[...], normed, NT)
    up_val = dot(su_ref[...], normed, NT)
    shared_ref[...] = (gate_val / (1.0 + jnp.exp(-gate_val)) * up_val).astype(BF16)


def route(tp_index, x, gain, routes_t, weight_t, sg_t, su_t, groups, local_experts, room, columns):
    tokens, width = x.shape
    slots = groups * room
    whole = pl.BlockSpec(memory_space=pltpu.VMEM)
    return pl.pallas_call(
        functools.partial(route_kernel, groups=groups, local_experts=local_experts, room=room),
        in_specs=[pl.BlockSpec(memory_space=pltpu.SMEM)] + [whole] * 6,
        out_specs=(whole, whole, whole),
        out_shape=(
            jax.ShapeDtypeStruct((slots, columns), BF16),
            jax.ShapeDtypeStruct((2, slots, tokens), BF16),
            jax.ShapeDtypeStruct((sg_t.shape[0], tokens), BF16),
        ),
        scratch_shapes=[pltpu.VMEM((tokens, width), BF16)],
        name="route",
    )(tp_index, x, gain, routes_t, weight_t, sg_t, su_t)


def by_expert(rows, count):
    own = lax.broadcasted_iota(jnp.int32, rows.shape, 0) % count
    return jnp.concatenate([jnp.where(own == e, rows, jnp.zeros((), rows.dtype)) for e in range(count)], axis=1)


def partial_kernel(rows_ref, w_ref, out_ref):
    peers, _, count, hidden, depth = w_ref.shape
    spread = by_expert(rows_ref[...], count)
    for g in range(2):
        w = jnp.concatenate([w_ref[:, g, e].reshape(peers * hidden, depth) for e in range(count)], axis=1)
        out_ref[:, g * peers * hidden : (g + 1) * peers * hidden] = dot(spread, w, NT).astype(BF16)


def partial_products(rows, weights):
    peers, _, count, hidden, _ = weights.shape
    return pl.pallas_call(
        partial_kernel,
        out_shape=jax.ShapeDtypeStruct((rows.shape[0], 2 * peers * hidden), BF16),
        name="partial",
    )(rows, weights)


def activate_kernel(parts_ref, out_ref):
    total = parts_ref[0].astype(F32)
    for t in range(1, parts_ref.shape[0]):
        total = total + parts_ref[t].astype(F32)
    half = out_ref.shape[1]
    gate_val = total[:, :half]
    out_ref[...] = (gate_val / (1.0 + jnp.exp(-gate_val)) * total[:, half:]).astype(BF16)


def activate(parts):
    _, rows, width = parts.shape
    return pl.pallas_call(
        activate_kernel,
        out_shape=jax.ShapeDtypeStruct((rows, width // 2), BF16),
        name="activate",
    )(parts)


def down_kernel(rows_ref, w_ref, out_ref):
    count, hidden, columns = w_ref.shape
    spread = by_expert(rows_ref[...], count)
    out_ref[...] = dot(spread, w_ref[...].reshape(count * hidden, columns)).astype(BF16)


def down(rows, weights):
    return pl.pallas_call(
        down_kernel,
        out_shape=jax.ShapeDtypeStruct((rows.shape[0], weights.shape[2]), BF16),
        name="down",
    )(rows, weights)


def combine_kernel(mix_ref, back_ref, shared_ref, w_ref, out_ref):
    back = back_ref[...]
    routed = dot(mix_ref[0], back, TN) + dot(mix_ref[1], back, TN)
    out_ref[...] = (routed + dot(shared_ref[...], w_ref[...], TN)).astype(BF16)


def combine(mix, back, shared, shared_down):
    return pl.pallas_call(
        combine_kernel,
        out_shape=jax.ShapeDtypeStruct((mix.shape[2], back.shape[1]), BF16),
        name="combine",
    )(mix, back, shared, shared_down)


def local(
    query_rows,
    key_rows,
    value_rows,
    cum_gate,
    out_weight,
    moe_input,
    moe_gain,
    routes,
    route_weight,
    expert_gate,
    expert_up,
    expert_down,
    shared_gate,
    shared_up,
    shared_down,
):
    groups = lax.axis_size("ep")
    peers = lax.axis_size("tp")
    ep_index = lax.axis_index("ep").astype(jnp.int32).reshape(1)
    tp_index = lax.axis_index("tp").astype(jnp.int32).reshape(1)
    local_experts = expert_gate.shape[0]
    columns = expert_down.shape[2]
    room = -(-CAP * local_experts // 8) * 8
    key_value = jnp.concatenate([key_rows.T, value_rows.T], axis=0)
    kv_all = lax.all_gather(key_value, "ep", axis=0)
    weights = lax.all_to_all(
        spread_weights(expert_gate.transpose(0, 2, 1), expert_up.transpose(0, 2, 1), peers).reshape(
            peers, -1, 128
        ),
        "tp", split_axis=0, concat_axis=0, tiled=True,
    )
    slots, mix, shared = route(
        tp_index, moe_input, moe_gain.reshape(1, -1), routes.T, route_weight.T, shared_gate.T, shared_up.T,
        groups, local_experts, room, columns,
    )
    arrived = lax.all_to_all(slots.reshape(groups, room, columns), "ep", split_axis=0, concat_axis=0, tiled=True)
    shared_all = sent_to_all(shared, "tp")
    parts = partial_products(
        arrived.reshape(groups * room, columns),
        weights.reshape(peers, 2, local_experts, expert_gate.shape[2], 128),
    )
    parts = lax.all_to_all(
        parts.reshape(peers, groups * room // peers, -1), "tp", split_axis=0, concat_axis=0, tiled=True
    )
    hidden = sent_to_all(activate(parts), "tp")
    result = down(hidden.reshape(groups * room, -1), expert_down)
    back = lax.all_to_all(result.reshape(groups, room, columns), "ep", split_axis=0, concat_axis=0, tiled=True)
    heads = attention(ep_index, query_rows.T, kv_all, cum_gate)
    mixer_out = projection(sent_to_all(heads, "tp"), out_weight)
    moe_out = combine(mix, back.reshape(groups * room, columns), shared_all.reshape(-1, shared_all.shape[2]), shared_down)
    return (mixer_out, moe_out)


def solution(mesh):
    placed = (
        P("ep", "tp"),
        P("ep", "tp"),
        P("ep", "tp"),
        P("tp", None),
        P(None, "tp"),
        P("ep", None),
        P(),
        P("ep", None),
        P("ep", None),
        P("ep", None, "tp"),
        P("ep", None, "tp"),
        P("ep", None, "tp"),
        P(None, "tp"),
        P(None, "tp"),
        P(None, "tp"),
    )
    return jax.shard_map(
        local, mesh=mesh, in_specs=placed, out_specs=(P("ep", "tp"), P("ep", "tp")), check_vma=False
    )
```

time: 559 us -> 260 us (0.47)
  the two profiles are of different devices: /device:TPU:1 before, /device:TPU:481 now
where the time goes in v1:
time: 260 us; the launch traced here: 259 us
  blocking collectives  92.3 us (36%)
  Pallas kernels  80.4 us (31%)
  waiting for transfers between devices  37.5 us (14%)
  starting transfers between devices  28 us (11%)
  between operations  14.1 us (5%)
  local copies, waits for them, and re-layouts  5.44 us (2%)
    pallas_call x1, Pallas kernels, attention(): pl.pallas_call(functools.partial(attention_kernel, tile=256), grid_spec=p...  57 us
    all_to_all x1, blocking collectives, local(): lax.all_to_all(parts.reshape(peers, groups * room // peers, -1), 'tp', sp...  37.3 us
    all_to_all x1, blocking collectives, local(): lax.all_to_all(slots.reshape(groups, room, columns), 'ep', split_axis=0,...  33.9 us
    all_to_all x2, waiting for transfers between devices, sent_to_all(): return lax.all_to_all(copies, axis, split_axis=0, concat_axis=0, tiled=True)  25.6 us
    all_to_all x1, blocking collectives, sent_to_all(): return lax.all_to_all(copies, axis, split_axis=0, concat_axis=0, tiled=True)  21.2 us
    all_to_all x1, starting transfers between devices, local(): lax.all_to_all(result.reshape(groups, room, columns), 'ep', split_axis=0,...  14 us
    all_to_all x1, waiting for transfers between devices, local(): lax.all_to_all(spread_weights(expert_gate.transpose(0, 2, 1), expert_up.t...  11.8 us
    all_to_all x2, starting transfers between devices, sent_to_all(): return lax.all_to_all(copies, axis, split_axis=0, concat_axis=0, tiled=True)  7.24 us
  transfers between devices with their start and end apart: 5, of which 3 were waited for; matrix products, arithmetic and copies ran while one was open for 1% of the time, Pallas kernels for 30%

profile of v1, /device:TPU:481, one launch (start us, length us, event | category | flops | bytes accessed | tf_op | source)
XLA Modules:
  0.0 259.4 jit_solution(109867015998232222)
XLA Ops:
  7.2 0.0 all-gather.3.cloned.1.call-start
  7.2 1.6 pad_maximum_fusion
  8.9 2.4 spread.1
  11.2 6.8 %all-to-all-start.2 = ((bf16[16,256,128]{2,1,0:T(8,128)(2,1)}), bf16[16,256,128]{2,1,0:T(8,128)(2,1)S(1)}, u32[]{:S(2)}, u32[]{:S(2)}) async-start(bf16[16,256,128]{2,1,0:T(8,128)(2,1)} %bitcast.24), calls=%async_computation.2 | async-start | bytes 2097152 | tf_op jit(solution)/shard_map/all_to_all | solution.py:307
  18.0 4.2 %route.1 = (bf16[1280,128]{1,0:T(8,128)(2,1)}, bf16[2,1280,192]{2,1,0:T(8,128)(2,1)}, bf16[32,192]{1,0:T(8,128)(2,1)}) custom-call(s32[1]{0:T(128)} %bitcast.5.tp_ref, bf16[192,2048]{1,0:T(8,128)(2,1)} %x_ref.1, f32[1,2048]{1,0:T(1,128)} %bitcast.37, s32[3,192]{1,0:T(4,128)} %bitcast.38, f32[3,192]{1,0:T(4,128)} %bitcast.39, bf16[32,2048]{1,0:T(8,128)(2,1)} %bitcast.33, ...), custom_call_target="tpu_custom_call" | custom-call | tf_op jit(solution)/shard_map/route/pallas_call | solution.py:199
  22.2 11.8 %all-to-all-done.2 = bf16[16,256,128]{2,1,0:T(8,128)(2,1)S(1)} async-done(((bf16[16,256,128]{2,1,0:T(8,128)(2,1)}), bf16[16,256,128]{2,1,0:T(8,128)(2,1)S(1)}, u32[]{:S(2)}, u32[]{:S(2)}) %all-to-all-start.2) | async-done | bytes 1048608 | tf_op jit(solution)/shard_map/all_to_all | solution.py:307
  34.1 33.9 %all_to_all.35 = bf16[32,40,128]{2,1,0:T(8,128)(2,1)} all-to-all(bf16[32,40,128]{2,1,0:T(8,128)(2,1)} %bitcast.32), channel_id=1, replica_groups=mesh['ep'=32,'tp'=16] {'ep'}, dimensions={0} | all-to-all | bytes 655360 | tf_op jit(solution)/shard_map/all_to_all | solution.py:317
  67.9 4.5 %partial.1 = bf16[1280,1024]{1,0:T(8,128)(2,1)} custom-call(bf16[1280,128]{1,0:T(8,128)(2,1)} %bitcast.28, bf16[16,2,4,32,128]{4,3,2,1,0:T(8,128)(2,1)} %bitcast.25), custom_call_target="tpu_custom_call" | custom-call | tf_op jit(solution)/shard_map/partial/pallas_call | solution.py:228
  72.4 37.3 %all_to_all.36.parts_ref = bf16[16,80,1024]{2,1,0:T(8,128)(2,1)} all-to-all(bf16[16,80,1024]{2,1,0:T(8,128)(2,1)} %bitcast.22), channel_id=1, replica_groups=mesh['ep'=32,'tp'=16] {'tp'}, dimensions={0} | all-to-all | bytes 5242880 | tf_op jit(solution)/shard_map/all_to_all | solution.py:323
  109.6 2.7 %activate.1 = bf16[80,512]{1,0:T(8,128)(2,1)} custom-call(bf16[16,80,1024]{2,1,0:T(8,128)(2,1)} %all_to_all.36.parts_ref), custom_call_target="tpu_custom_call" | custom-call | tf_op jit(solution)/shard_map/activate/pallas_call | solution.py:246
  112.4 1.0 broadcast_in_dim.10
  113.4 21.2 %all_to_all.37 = bf16[16,80,512]{2,1,0:T(8,128)(2,1)} all-to-all(bf16[16,80,512]{2,1,0:T(8,128)(2,1)S(1)} %broadcast_in_dim.10), channel_id=1, replica_groups=mesh['ep'=32,'tp'=16] {'tp'}, dimensions={0} | all-to-all | bytes 2621440 | tf_op jit(solution)/shard_map/all_to_all | solution.py:28
  134.6 0.8 broadcast_in_dim.11
  135.4 3.5 %all-to-all-start.6 = ((bf16[16,32,192]{2,1,0:T(8,128)(2,1)}), bf16[16,32,192]{2,1,0:T(8,128)(2,1)S(1)}, u32[]{:S(2)}, u32[]{:S(2)}) async-start(bf16[16,32,192]{2,1,0:T(8,128)(2,1)} %broadcast_in_dim.11), calls=%async_computation.6 | async-start | bytes 524288 | tf_op jit(solution)/shard_map/all_to_all | solution.py:28
  138.9 3.7 %down.1 = bf16[1280,128]{1,0:T(8,128)(2,1)} custom-call(bf16[1280,512]{1,0:T(8,128)(2,1)} %bitcast.23, bf16[4,512,128]{2,1,0:T(8,128)(2,1)} %w_ref.4), custom_call_target="tpu_custom_call" | custom-call | tf_op jit(solution)/shard_map/down/pallas_call | solution.py:260
  142.6 3.8 %all-to-all-done.6 = bf16[16,32,192]{2,1,0:T(8,128)(2,1)S(1)} async-done(((bf16[16,32,192]{2,1,0:T(8,128)(2,1)}), bf16[16,32,192]{2,1,0:T(8,128)(2,1)S(1)}, u32[]{:S(2)}, u32[]{:S(2)}) %all-to-all-start.6) | async-done | bytes 196640 | tf_op jit(solution)/shard_map/all_to_all | solution.py:28
  146.4 14.0 %all-to-all-start.5 = ((bf16[32,40,128]{2,1,0:T(8,128)(2,1)}), bf16[32,40,128]{2,1,0:T(8,128)(2,1)S(1)}, u32[]{:S(2)}, u32[]{:S(2)}) async-start(bf16[32,40,128]{2,1,0:T(8,128)(2,1)} %bitcast.27), calls=%async_computation.5 | async-start | bytes 655360 | tf_op jit(solution)/shard_map/all_to_all | solution.py:328
  160.5 57.0 %attention.1 = bf16[384,128]{1,0:T(8,128)(2,1)} custom-call(s32[1]{0:T(128)} %bitcast.ep_ref, bf16[64,768]{1,0:T(8,128)(2,1)} %bitcast.41, bf16[32,128,768]{2,1,0:T(8,128)(2,1)} %bitcast.40, f32[1,24576]{1,0:T(1,128)} %g0_ref.1, f32[1,24576]{1,0:T(1,128)} %g0_ref.1), custom_call_target="tpu_custom_call" | custom-call | flops 19327352832 | bytes 8388608 | tf_op jit(solution)/shard_map/attention/pallas_call | solution.py:91
  217.5 2.5 broadcast_in_dim.9
  220.0 3.7 %all-to-all-start = ((bf16[16,384,128]{2,1,0:T(8,128)(2,1)}), bf16[16,384,128]{2,1,0:T(8,128)(2,1)S(1)}, u32[]{:S(2)}, u32[]{:S(2)}) async-start(bf16[16,384,128]{2,1,0:T(8,128)(2,1)} %broadcast_in_dim.9), calls=%async_computation | async-start | bytes 3145728 | tf_op jit(solution)/shard_map/all_to_all | solution.py:28
  223.7 2.8 %combine.1 = bf16[192,128]{1,0:T(8,128)(2,1)} custom-call(bf16[2,1280,192]{2,1,0:T(8,128)(2,1)} %get-tuple-element.5.mix_ref, bf16[1280,128]{1,0:T(8,128)(2,1)} %bitcast.26, bf16[512,192]{1,0:T(8,128)(2,1)} %bitcast.29, bf16[512,128]{1,0:T(8,128)(2,1)} %w_ref.5), custom_call_target="tpu_custom_call" | custom-call | tf_op jit(solution)/shard_map/combine/pallas_call | solution.py:274
  226.5 21.8 %all-to-all-done.heads_ref = bf16[16,384,128]{2,1,0:T(8,128)(2,1)S(1)} async-done(((bf16[16,384,128]{2,1,0:T(8,128)(2,1)}), bf16[16,384,128]{2,1,0:T(8,128)(2,1)S(1)}, u32[]{:S(2)}, u32[]{:S(2)}) %all-to-all-start) | async-done | bytes 1572896 | tf_op jit(solution)/shard_map/all_to_all | solution.py:28
  248.3 1.2 copy-done
  249.5 3.1 %projection.1 = bf16[768,128]{1,0:T(8,128)(2,1)} custom-call(bf16[16,384,128]{2,1,0:T(8,128)(2,1)} %copy-done, bf16[1024,128]{1,0:T(8,128)(2,1)} %w_ref.3), custom_call_target="tpu_custom_call" | custom-call | flops 402653184 | bytes 4194304 | tf_op jit(solution)/shard_map/projection/pallas_call | solution.py:133
  (12 shorter events, 0.1 us)
Async XLA Ops:
  7.2 153.3 %all-gather.3.cloned.1.call-start = ((), (), s32[]{:S(2)}) async-start(), calls=%async_computation.7 | async-start | bytes 6488064 | tf_op jit(solution)/shard_map/all_gather | solution.py:306
  11.2 22.8 %all-to-all-start.2 = ((bf16[16,256,128]{2,1,0:T(8,128)(2,1)}), bf16[16,256,128]{2,1,0:T(8,128)(2,1)S(1)}, u32[]{:S(2)}, u32[]{:S(2)}) async-start(bf16[16,256,128]{2,1,0:T(8,128)(2,1)} %bitcast.24), calls=%async_computation.2 | async-start | bytes 2097152 | tf_op jit(solution)/shard_map/all_to_all | solution.py:307
  34.0 33.9 %copy-start.1 = (bf16[16,256,128]{2,1,0:T(8,128)(2,1)}, bf16[16,256,128]{2,1,0:T(8,128)(2,1)S(1)}, u32[]{:S(2)}) copy-start(bf16[16,256,128]{2,1,0:T(8,128)(2,1)S(1)} %all-to-all-done.2) | copy-start | bytes 3145732
  113.4 21.2 %copy-start.4 = (bf16[32,192]{1,0:T(8,128)(2,1)S(1)}, bf16[32,192]{1,0:T(8,128)(2,1)}, u32[]{:S(2)}) copy-start(bf16[32,192]{1,0:T(8,128)(2,1)} %get-tuple-element.7) | copy-start | bytes 36868
  135.4 11.0 %all-to-all-start.6 = ((bf16[16,32,192]{2,1,0:T(8,128)(2,1)}), bf16[16,32,192]{2,1,0:T(8,128)(2,1)S(1)}, u32[]{:S(2)}, u32[]{:S(2)}) async-start(bf16[16,32,192]{2,1,0:T(8,128)(2,1)} %broadcast_in_dim.11), calls=%async_computation.6 | async-start | bytes 524288 | tf_op jit(solution)/shard_map/all_to_all | solution.py:28
  146.4 71.1 %copy-start.3 = (bf16[16,32,192]{2,1,0:T(8,128)(2,1)}, bf16[16,32,192]{2,1,0:T(8,128)(2,1)S(1)}, u32[]{:S(2)}) copy-start(bf16[16,32,192]{2,1,0:T(8,128)(2,1)S(1)} %all-to-all-done.6) | copy-start | bytes 589828
  146.4 71.1 %all-to-all-start.5 = ((bf16[32,40,128]{2,1,0:T(8,128)(2,1)}), bf16[32,40,128]{2,1,0:T(8,128)(2,1)S(1)}, u32[]{:S(2)}, u32[]{:S(2)}) async-start(bf16[32,40,128]{2,1,0:T(8,128)(2,1)} %bitcast.27), calls=%async_computation.5 | async-start | bytes 655360 | tf_op jit(solution)/shard_map/all_to_all | solution.py:328
  217.5 2.5 copy-start.2
  220.0 28.3 %all-to-all-start = ((bf16[16,384,128]{2,1,0:T(8,128)(2,1)}), bf16[16,384,128]{2,1,0:T(8,128)(2,1)S(1)}, u32[]{:S(2)}, u32[]{:S(2)}) async-start(bf16[16,384,128]{2,1,0:T(8,128)(2,1)} %broadcast_in_dim.9), calls=%async_computation | async-start | bytes 3145728 | tf_op jit(solution)/shard_map/all_to_all | solution.py:28
  248.3 1.2 copy-start
Sparse Core Ops, SparseCore 0:
  10.7 84.6 all-gather.2

commit v2 on v1

v2 whole, which is shorter than its diff:
```python
import functools
import math

import jax
import jax.numpy as jnp
from jax import lax
from jax.experimental import pallas as pl
from jax.experimental.pallas import tpu as pltpu
from jax.sharding import PartitionSpec as P

HEAD = 64
CAP = 9
LOG2E = 1.4426950408889634
neg_fill = -1e30
norm_eps = 1e-06
F32 = jnp.float32
BF16 = jnp.bfloat16
NT = (((1,), (1,)), ((), ()))
TN = (((0,), (0,)), ((), ()))
NN = (((1,), (0,)), ((), ()))


def dot(a, b, dims=NN):
    return lax.dot_general(a, b, dims, preferred_element_type=F32)


def exchanged(array, axis, among=None):
    return lax.all_to_all(array, axis, split_axis=0, concat_axis=0, tiled=True, axis_index_groups=among)


def sent_to_all(array, axis, among=None):
    count = len(among[0]) if among else lax.axis_size(axis)
    return exchanged(jnp.broadcast_to(array, (count, *array.shape)), axis, among)


def cost(flops, nbytes):
    return pl.CostEstimate(flops=flops, transcendentals=0, bytes_accessed=nbytes)


HEADROOM = 64.0
EXTRA = 16


def three(x):
    first = x.astype(BF16)
    rest = x - first.astype(F32)
    second = rest.astype(BF16)
    return first, second, (rest - second.astype(F32)).astype(BF16)


def attention_kernel(ep_ref, *refs, tile, opening):
    if opening:
        q_ref, kv_ref, gk_ref, g0_ref, _, acc_out, m_out, q_scr, m_scr, acc_scr = refs
    else:
        q_ref, kv_ref, gk_ref, g0_ref, acc_in, m_in, _, out_ref, q_scr, m_scr, acc_scr = refs
    step = pl.program_id(0)
    own = ep_ref[0]
    count = own // 2 if opening else own - own // 2
    rows = q_scr.shape[0]
    keys = kv_ref.shape[2]

    def operands():
        kt = kv_ref[0, :HEAD, :]
        row_id = lax.broadcasted_iota(jnp.int32, (2 * HEAD, keys), 0)
        vt = jnp.where(row_id < HEAD, jnp.ones((), BF16), kv_ref[0])
        gate = (gk_ref[...] - g0_ref[:, :1]) * LOG2E
        row_id = lax.broadcasted_iota(jnp.int32, (EXTRA, keys), 0)
        gates = jnp.zeros((EXTRA, keys), F32)
        for n, piece in enumerate(three(gate)):
            gates = jnp.where(row_id == n, piece.astype(F32), gates)
        return jnp.concatenate([kt, kt, kt, gates.astype(BF16)], axis=0), vt

    def exact(source, target, diagonal):
        kx, vt = operands()
        for i in range(rows // tile):
            span = pl.ds(i * tile, tile)
            used = min(keys, (i + 1) * tile) if diagonal else keys
            s = dot(q_scr[span, :], kx[:, :used])
            if diagonal:
                q_pos = i * tile + lax.broadcasted_iota(jnp.int32, (tile, used), 0)
                k_pos = lax.broadcasted_iota(jnp.int32, (tile, used), 1)
                s = jnp.where(k_pos <= q_pos, s, neg_fill)
            top = jnp.max(s, axis=1, keepdims=True)
            if diagonal:
                p = jnp.exp2(s - top).astype(BF16)
                acc_scr[target, span, :] = dot(p, vt[:, :used], NT)
                m_scr[span, :] = jnp.broadcast_to(top, (tile, m_scr.shape[1]))
            else:
                old = m_scr[span, :]
                new = jnp.maximum(old, top)
                p = jnp.exp2(s - new[:, :1]).astype(BF16)
                acc_scr[target, span, :] = acc_scr[source, span, :] * jnp.exp2(old - new) + dot(p, vt, NT)
                m_scr[span, :] = new

    @pl.when(step == 0)
    def _():
        for n, piece in enumerate(three(q_ref[...].T.astype(F32) * (LOG2E * HEAD**-0.5))):
            q_scr[:, n * HEAD : (n + 1) * HEAD] = piece
        q_scr[:, 3 * HEAD :] = jnp.full((rows, EXTRA), -1.0, BF16)
        if opening:
            exact(0, 0, True)
        else:
            acc_scr[0] = acc_in[...]
            m_scr[...] = m_in[...]

    @pl.when((step > 0) & (step <= count))
    def _():
        source = (step - 1) % 2
        target = step % 2
        kx, vt = operands()
        worst = jnp.full((8, 128), neg_fill, F32)
        for i in range(rows // tile):
            span = pl.ds(i * tile, tile)
            x = dot(q_scr[span, :], kx) - m_scr[span, :1]
            most = x[:, :128]
            for c in range(128, keys, 128):
                most = jnp.maximum(most, x[:, c : c + 128])
            worst = jnp.maximum(worst, jnp.max(most.reshape(tile // 8, 8, 128), axis=0))
            acc_scr[target, span, :] = acc_scr[source, span, :] + dot(jnp.exp2(x).astype(BF16), vt, NT)

        @pl.when(jnp.max(worst) > HEADROOM)
        def _():
            exact(source, target, False)

    @pl.when(step == pl.num_programs(0) - 1)
    def _():
        last = count % 2
        if opening:
            acc_out[...] = acc_scr[last]
            m_out[...] = m_scr[...]
        else:
            half = rows // 2
            top = acc_scr[last, :half, :]
            low = acc_scr[last, half:, :]
            out_ref[...] = jnp.concatenate(
                [top[:, HEAD:] / top[:, :HEAD], low[:, HEAD:] / low[:, :HEAD]], axis=1
            ).astype(BF16)


def attention(ep_index, q_t, kv_all, cum_gate, state, after):
    blocks, wide, keys = kv_all.shape
    rows = q_t.shape[1]
    opening = state is None

    def place(j, ep):
        own = ep[0]
        half = own // 2
        if opening:
            return jnp.where(j == 0, own, jnp.maximum(jnp.minimum(j, half) - 1, 0))
        return jnp.minimum(half + jnp.maximum(j - 1, 0), jnp.maximum(own - 1, 0))

    flat = pl.BlockSpec((rows, 128), lambda j, ep: (0, 0))
    wide_f32 = jax.ShapeDtypeStruct((rows, 128), F32)
    return pl.pallas_call(
        functools.partial(attention_kernel, tile=384, opening=opening),
        grid_spec=pltpu.PrefetchScalarGridSpec(
            num_scalar_prefetch=1,
            grid=(blocks // 2 + (0 if opening else 1),),
            in_specs=[
                pl.BlockSpec((HEAD, rows), lambda j, ep: (0, 0)),
                pl.BlockSpec((1, wide, keys), lambda j, ep: (place(j, ep), 0, 0)),
                pl.BlockSpec((1, keys), lambda j, ep: (0, place(j, ep))),
                pl.BlockSpec((1, keys), lambda j, ep: (0, ep[0])),
            ]
            + ([] if opening else [flat, flat])
            + [pl.BlockSpec(memory_space=pl.ANY)],
            out_specs=(flat, flat) if opening else pl.BlockSpec((rows // 2, 2 * HEAD), lambda j, ep: (0, 0)),
            scratch_shapes=[
                pltpu.VMEM((rows, 3 * HEAD + EXTRA), BF16),
                pltpu.VMEM((rows, 128), F32),
                pltpu.VMEM((2, rows, 128), F32),
            ],
        ),
        out_shape=(wide_f32, wide_f32) if opening else jax.ShapeDtypeStruct((rows // 2, 2 * HEAD), BF16),
        compiler_params=pltpu.CompilerParams(dimension_semantics=("arbitrary",)),
        cost_estimate=cost(2 * rows * keys * blocks * 256, 4 << 20),
        name="attention_first" if opening else "attention_rest",
    )(ep_index, q_t, kv_all, cum_gate, cum_gate, *(state or ()), after)


def projection_kernel(heads_ref, w_ref, out_ref):
    count, half, _ = heads_ref.shape
    acc = jnp.zeros((half, 2 * w_ref.shape[1]), F32)
    blank = jnp.zeros((HEAD, w_ref.shape[1]), BF16)
    for h in range(count):
        w = w_ref[h * HEAD : (h + 1) * HEAD, :]
        both = jnp.concatenate(
            [jnp.concatenate([w, blank], axis=1), jnp.concatenate([blank, w], axis=1)], axis=0
        )
        acc = acc + dot(heads_ref[h], both)
    out_ref[:half, :] = acc[:, : w_ref.shape[1]].astype(BF16)
    out_ref[half:, :] = acc[:, w_ref.shape[1] :].astype(BF16)


def projection(heads, out_weight):
    count, half, _ = heads.shape
    columns = out_weight.shape[1]
    return pl.pallas_call(
        projection_kernel,
        out_shape=jax.ShapeDtypeStruct((2 * half, columns), BF16),
        cost_estimate=cost(2 * half * count * 128 * 256, 4 << 20),
        name="projection",
    )(heads, out_weight)


def spread_kernel(side_ref, gate_ref, up_ref, sg_ref, su_ref, *out_refs):
    side = len(out_refs)
    experts, hidden, width = gate_ref.shape
    part = width // side
    block = experts * hidden
    for k, out_ref in enumerate(out_refs):
        lanes = pl.ds(pl.multiple_of(lax.rem(side_ref[1] + k, side) * part, part), part)
        out_ref[:block, :] = gate_ref[:, :, lanes].reshape(block, part)
        out_ref[block : 2 * block, :] = up_ref[:, :, lanes].reshape(block, part)
        out_ref[2 * block : 2 * block + hidden, :] = sg_ref[:, lanes]
        out_ref[2 * block + hidden :, :] = su_ref[:, lanes]


def spread_weights(side_index, gate_t, up_t, sg_t, su_t, side):
    experts, hidden, width = gate_t.shape
    whole = pl.BlockSpec(memory_space=pltpu.VMEM)
    rows = 2 * (experts + 1) * hidden
    return pl.pallas_call(
        spread_kernel,
        in_specs=[pl.BlockSpec(memory_space=pltpu.SMEM)] + [whole] * 4,
        out_specs=[whole] * side,
        out_shape=[jax.ShapeDtypeStruct((rows, width // side), BF16)] * side,
        name="spread",
    )(side_index, gate_t, up_t, sg_t, su_t)


def route_kernel(
    side_ref, x_ref, gain_ref, routes_ref, weight_ref, slot_ref, mix_ref, part_ref, norm_scr,
    *, side, groups, local_experts, room,
):
    tokens = x_ref.shape[0]
    x = x_ref[...].astype(F32)
    scale = lax.rsqrt(jnp.mean(x * x, axis=1, keepdims=True) + norm_eps)
    norm_scr[...] = (x * scale * gain_ref[...]).astype(BF16)
    columns = slot_ref.shape[1]
    wide = part_ref.shape[1]
    part_ref[...] = norm_scr[:, pl.ds(pl.multiple_of(side_ref[1] * wide, wide), wide)]
    start = pl.multiple_of((side_ref[1] * side + side_ref[0]) * columns, columns)
    piece = norm_scr[:, pl.ds(start, columns)]
    slots = groups * room
    shape = (groups, room, tokens)
    within = lax.broadcasted_iota(jnp.int32, shape, 1)
    expert = lax.broadcasted_iota(jnp.int32, shape, 0) * local_experts + within % local_experts
    expert = expert.reshape(slots, tokens)
    turn = (within // local_experts).reshape(slots, tokens).astype(F32)
    hit = jnp.zeros((slots, tokens), F32)
    weight = jnp.zeros((slots, tokens), F32)
    for j in range(routes_ref.shape[0]):
        same = expert == routes_ref[j : j + 1, :]
        hit = hit + jnp.where(same, 1.0, 0.0)
        weight = weight + jnp.where(same, weight_ref[j : j + 1, :], 0.0)
    before = lax.broadcasted_iota(jnp.int32, (tokens, tokens), 0)
    after = lax.broadcasted_iota(jnp.int32, (tokens, tokens), 1)
    earlier = jnp.where(before < after, 1.0, 0.0).astype(BF16)
    rank = dot(hit.astype(BF16), earlier)
    chosen = jnp.where(rank == turn, hit, 0.0)
    slot_ref[...] = dot(chosen.astype(BF16), piece).astype(BF16)
    mix = chosen * weight
    coarse = mix.astype(BF16)
    mix_ref[0] = coarse
    mix_ref[1] = (mix - coarse.astype(F32)).astype(BF16)


def route(side_index, x, gain, routes_t, weight_t, side, groups, local_experts, room, columns):
    tokens, width = x.shape
    slots = groups * room
    whole = pl.BlockSpec(memory_space=pltpu.VMEM)
    return pl.pallas_call(
        functools.partial(route_kernel, side=side, groups=groups, local_experts=local_experts, room=room),
        in_specs=[pl.BlockSpec(memory_space=pltpu.SMEM)] + [whole] * 4,
        out_specs=(whole, whole, whole),
        out_shape=(
            jax.ShapeDtypeStruct((slots, columns), BF16),
            jax.ShapeDtypeStruct((2, slots, tokens), BF16),
            jax.ShapeDtypeStruct((tokens, width // side), BF16),
        ),
        scratch_shapes=[pltpu.VMEM((tokens, width), BF16)],
        name="route",
    )(side_index, x, gain, routes_t, weight_t)


def by_expert(rows, count):
    own = lax.broadcasted_iota(jnp.int32, rows.shape, 0) % count
    return jnp.concatenate([jnp.where(own == e, rows, jnp.zeros((), rows.dtype)) for e in range(count)], axis=1)


def partial_kernel(side_ref, rows_ref, tokens_ref, *refs, count, hidden):
    side = len(refs) - 3
    out_ref, w_scr, shared_scr = refs[side:]
    wide = side * hidden
    depth = rows_ref.shape[2]
    for k in range(side):
        place = pl.multiple_of(lax.rem(side_ref[1] + side - k, side) * hidden, hidden)
        for g in range(2):
            span = pl.ds(g * wide + place, hidden)
            for e in range(count):
                first = (g * count + e) * hidden
                for c in range(side):
                    lanes = (c * count + e) * depth
                    w_scr[span, lanes : lanes + depth] = refs[k][first : first + hidden, c * depth : (c + 1) * depth]
            first = (2 * count + g) * hidden
            shared_scr[span, :] = refs[k][first : first + hidden, :]
    each = rows_ref.shape[1] // side
    few = tokens_ref.shape[0] // side
    for n in range(side):
        total = jnp.zeros((each, 2 * wide), F32)
        for c in range(side):
            spread = by_expert(rows_ref[c, n * each : (n + 1) * each, :], count)
            total = total + dot(spread, w_scr[:, c * count * depth : (c + 1) * count * depth], NT)
        out_ref[n, :each, :] = total.astype(BF16)
        out_ref[n, each:, :] = dot(tokens_ref[n * few : (n + 1) * few, :], shared_scr[...], NT).astype(BF16)


def partial_products(side_index, rows, tokens, weights, count, hidden):
    side = len(weights)
    whole = pl.BlockSpec(memory_space=pltpu.VMEM)
    each = (rows.shape[1] + tokens.shape[0]) // side
    return pl.pallas_call(
        functools.partial(partial_kernel, count=count, hidden=hidden),
        in_specs=[pl.BlockSpec(memory_space=pltpu.SMEM)] + [whole] * (2 + side),
        out_specs=whole,
        out_shape=jax.ShapeDtypeStruct((side, each, 2 * side * hidden), BF16),
        scratch_shapes=[
            pltpu.VMEM((2 * side * hidden, count * side * rows.shape[2]), BF16),
            pltpu.VMEM((2 * side * hidden, tokens.shape[1]), BF16),
        ],
        name="partial",
    )(side_index, rows, tokens, *weights)


def activate_kernel(parts_ref, out_ref):
    total = parts_ref[0].astype(F32)
    for t in range(1, parts_ref.shape[0]):
        total = total + parts_ref[t].astype(F32)
    half = out_ref.shape[1]
    gate_val = total[:, :half]
    out_ref[...] = (gate_val / (1.0 + jnp.exp(-gate_val)) * total[:, half:]).astype(BF16)


def activate(parts):
    _, rows, width = parts.shape
    return pl.pallas_call(
        activate_kernel,
        out_shape=jax.ShapeDtypeStruct((rows, width // 2), BF16),
        name="activate",
    )(parts)


def down_kernel(hidden_ref, w_ref, sw_ref, out_ref, shared_ref, *, side):
    count, hidden, columns = w_ref.shape
    each = out_ref.shape[0] // side
    few = shared_ref.shape[0] // side
    w = w_ref[...].reshape(count * hidden, columns)
    for n in range(side):
        rows = jnp.concatenate([hidden_ref[y * side + n] for y in range(side)], axis=1)
        out_ref[n * each : (n + 1) * each, :] = dot(by_expert(rows[:each], count), w).astype(BF16)
        shared_ref[n * few : (n + 1) * few, :] = dot(rows[each:], sw_ref[...])


def down(hidden, weights, shared_down, side, slots):
    columns = weights.shape[2]
    whole = pl.BlockSpec(memory_space=pltpu.VMEM)
    return pl.pallas_call(
        functools.partial(down_kernel, side=side),
        in_specs=[whole] * 3,
        out_specs=(whole, whole),
        out_shape=(
            jax.ShapeDtypeStruct((slots, columns), BF16),
            jax.ShapeDtypeStruct((hidden.shape[1] * side - slots, columns), F32),
        ),
        name="down",
    )(hidden, weights, shared_down)


def combine_kernel(mix_ref, back_ref, shared_ref, out_ref):
    back = back_ref[...]
    routed = dot(mix_ref[0], back, TN) + dot(mix_ref[1], back, TN)
    out_ref[...] = (routed + shared_ref[...]).astype(BF16)


def combine(mix, back, shared):
    return pl.pallas_call(
        combine_kernel,
        out_shape=jax.ShapeDtypeStruct((mix.shape[2], back.shape[1]), BF16),
        name="combine",
    )(mix, back, shared)


def local(
    query_rows,
    key_rows,
    value_rows,
    cum_gate,
    out_weight,
    moe_input,
    moe_gain,
    routes,
    route_weight,
    expert_gate,
    expert_up,
    expert_down,
    shared_gate,
    shared_up,
    shared_down,
):
    groups = lax.axis_size("ep")
    peers = lax.axis_size("tp")
    side = math.isqrt(peers)
    along_x = [[y * side + x for x in range(side)] for y in range(side)]
    along_y = [[y * side + x for y in range(side)] for x in range(side)]
    ep_index = lax.axis_index("ep").astype(jnp.int32).reshape(1)
    tp_index = lax.axis_index("tp").astype(jnp.int32)
    side_index = jnp.stack([tp_index // side, tp_index % side])
    local_experts, _, hidden_each = expert_gate.shape
    columns = expert_down.shape[2]
    room = -(-CAP * local_experts // 8) * 8
    slot_count = groups * room
    key_value = jnp.concatenate([key_rows.T, value_rows.T], axis=0)
    kv_all = lax.all_gather(key_value, "ep", axis=0)
    slots, mix, tokens = route(
        side_index, moe_input, moe_gain.reshape(1, -1), routes.T, route_weight.T,
        side, groups, local_experts, room, columns,
    )
    arrived = exchanged(slots.reshape(groups, room, columns), "ep")
    pieces = spread_weights(
        side_index, expert_gate.transpose(0, 2, 1), expert_up.transpose(0, 2, 1), shared_gate.T, shared_up.T, side
    )
    pieces = [pieces[0]] + [
        lax.ppermute(
            pieces[k], "tp", [(row[x], row[(x + k) % side]) for row in along_x for x in range(side)]
        )
        for k in range(1, side)
    ]
    gathered = sent_to_all(arrived.reshape(slot_count, columns), "tp", along_y)
    parts = partial_products(side_index, gathered, tokens, pieces, local_experts, hidden_each)
    parts = exchanged(parts, "tp", along_x)
    own_hidden = activate(parts)
    hidden = sent_to_all(own_hidden, "tp")
    state = attention(ep_index, query_rows.T, kv_all, cum_gate, None, own_hidden)
    result, shared = down(hidden, expert_down, shared_down, side, slot_count)
    back = exchanged(result.reshape(groups, room, columns), "ep")
    heads = attention(ep_index, query_rows.T, kv_all, cum_gate, state, result)
    heads = sent_to_all(heads, "tp")
    mixer_out = projection(heads, out_weight)
    moe_out = combine(mix, back.reshape(slot_count, columns), shared)
    return (mixer_out, moe_out)


def solution(mesh):
    placed = (
        P("ep", "tp"),
        P("ep", "tp"),
        P("ep", "tp"),
        P("tp", None),
        P(None, "tp"),
        P("ep", None),
        P(),
        P("ep", None),
        P("ep", None),
        P("ep", None, "tp"),
        P("ep", None, "tp"),
        P("ep", None, "tp"),
        P(None, "tp"),
        P(None, "tp"),
        P(None, "tp"),
    )
    return jax.shard_map(
        local, mesh=mesh, in_specs=placed, out_specs=(P("ep", "tp"), P("ep", "tp")), check_vma=False
    )
```

time: 260 us -> 264 us (1.015)
  blocking collectives: 92.3 us -> 48 us
  waiting for transfers between devices: 37.5 us -> 55.5 us
  starting transfers between devices: 28 us -> 44 us
  Pallas kernels: 80.4 us -> 89.4 us
  local copies, waits for them, and re-layouts: 5.44 us -> 9.32 us
    all_to_all x3 -> x2, blocking collectives: 92.3 us -> 48 us  [exchanged(): lax.all_to_all(array, axis, split_axis=0, concat_axis=0, tiled=True, axis...]
    ppermute x0 -> x3, starting transfers between devices: none -> 10.5 us  [local(): lax.ppermute(pieces[k], 'tp', [(row[x], row[(x + k) % side]) for row in a...]
    pallas_call x5 -> x6, Pallas kernels: 71.8 us -> 81.9 us  [the longest x2 66.6 us: attention(): pl.pallas_call(functools.partial(attention_kernel, tile=384, opening=open...]
    ppermute x0 -> x3, waiting for transfers between devices: none -> 10.1 us  [local(): lax.ppermute(pieces[k], 'tp', [(row[x], row[(x + k) % side]) for row in a...]
    all_to_all x4, waiting for transfers between devices: 37.5 us -> 45.4 us  [exchanged(): lax.all_to_all(array, axis, split_axis=0, concat_axis=0, tiled=True, axis...]
    all_to_all x4, starting transfers between devices: 28 us -> 33.5 us  [exchanged(): lax.all_to_all(array, axis, split_axis=0, concat_axis=0, tiled=True, axis...]
  transfers between devices with their start and end apart: 5 -> 8, of which waited for: 3 -> 5; matrix products, arithmetic and copies ran while one was open for 1% -> 2% of each run, Pallas kernels for 30% -> 33%
where the time goes in v2:
time: 264 us; the launch traced here: 263 us
  Pallas kernels  89.4 us (34%)
  waiting for transfers between devices  55.5 us (21%)
  blocking collectives  48 us (18%)
  starting transfers between devices  44 us (17%)
  between operations  14.1 us (5%)
  local copies, waits for them, and re-layouts  9.32 us (4%)
    pallas_call x2, Pallas kernels, attention(): pl.pallas_call(functools.partial(attention_kernel, tile=384, opening=open...  66.6 us
    all_to_all x2, blocking collectives, exchanged(): lax.all_to_all(array, axis, split_axis=0, concat_axis=0, tiled=True, axis...  48 us
    all_to_all x4, waiting for transfers between devices, exchanged(): lax.all_to_all(array, axis, split_axis=0, concat_axis=0, tiled=True, axis...  45.4 us
    all_to_all x4, starting transfers between devices, exchanged(): lax.all_to_all(array, axis, split_axis=0, concat_axis=0, tiled=True, axis...  33.5 us
    ppermute x3, starting transfers between devices, local(): lax.ppermute(pieces[k], 'tp', [(row[x], row[(x + k) % side]) for row in a...  10.5 us
    ppermute x3, waiting for transfers between devices, local(): lax.ppermute(pieces[k], 'tp', [(row[x], row[(x + k) % side]) for row in a...  10.1 us
    broadcast_in_dim x3, local copies, waits for them, and re-layouts, sent_to_all(): jnp.broadcast_to(array, (count, *array.shape))  5.89 us
  transfers between devices with their start and end apart: 8, of which 5 were waited for; matrix products, arithmetic and copies ran while one was open for 2% of the time, Pallas kernels for 33%

profile of v2, /device:TPU:481, one launch (start us, length us, event | category | flops | bytes accessed | tf_op | source)
XLA Modules:
  0.0 262.7 jit_solution(16276115337516978994)
XLA Ops:
  9.5 4.2 %route.1 = (bf16[1280,128]{1,0:T(8,128)(2,1)}, bf16[2,1280,192]{2,1,0:T(8,128)(2,1)}, bf16[192,512]{1,0:T(8,128)(2,1)}) custom-call(s32[2]{0:T(128)} %pad_add_fusion.side_ref, bf16[192,2048]{1,0:T(8,128)(2,1)} %x_ref.1, f32[1,2048]{1,0:T(1,128)} %bitcast.28, s32[3,192]{1,0:T(4,128)} %bitcast.29, f32[3,192]{1,0:T(4,128)} %bitcast.30), custom_call_target="tpu_custom_call" | custom-call | tf_op jit(solution)/shard_map/route/pallas_call | solution.py:273
  13.8 31.2 %all_to_all.30 = bf16[32,40,128]{2,1,0:T(8,128)(2,1)S(1)} all-to-all(bf16[32,40,128]{2,1,0:T(8,128)(2,1)} %bitcast.23), channel_id=1, replica_groups=mesh['ep'=32,'tp'=16] {'ep'}, dimensions={0} | all-to-all | bytes 655360 | tf_op jit(solution)/shard_map/all_to_all | solution.py:28
  46.2 4.0 %all-to-all-start.1 = ((bf16[4,1280,128]{2,1,0:T(8,128)(2,1)}), bf16[4,1280,128]{2,1,0:T(8,128)(2,1)S(1)}, u32[]{:S(2)}, u32[]{:S(2)}) async-start(bf16[4,1280,128]{2,1,0:T(8,128)(2,1)} %broadcast_in_dim.9), calls=%async_computation.1 | async-start | bytes 2621440 | tf_op jit(solution)/shard_map/all_to_all | solution.py:28
  50.2 2.4 spread.1
  52.6 3.1 %collective-permute-start = (bf16[320,512]{1,0:T(8,128)(2,1)}, bf16[320,512]{1,0:T(8,128)(2,1)S(1)}, u32[]{:S(2)}, u32[]{:S(2)}) collective-permute-start(bf16[320,512]{1,0:T(8,128)(2,1)} %get-tuple-element.16), channel_id=1, source_target_pairs={{0,1},{1,2},{2,3},{3,0},{4,5},{5,6},{6,7},{7,4},{8,9},{9,10},{10,1... | collective-permute-start | bytes 983048 | tf_op jit(solution)/shard_map/ppermute | solution.py:434
  55.7 4.3 %collective-permute-start.1 = (bf16[320,512]{1,0:T(8,128)(2,1)}, bf16[320,512]{1,0:T(8,128)(2,1)S(1)}, u32[]{:S(2)}, u32[]{:S(2)}) collective-permute-start(bf16[320,512]{1,0:T(8,128)(2,1)} %get-tuple-element.17), channel_id=1, source_target_pairs={{0,2},{1,3},{2,0},{3,1},{4,6},{5,7},{6,4},{7,5},{8,10},{9,11},{10,... | collective-permute-start | bytes 983048 | tf_op jit(solution)/shard_map/ppermute | solution.py:434
  60.1 3.1 %collective-permute-start.2 = (bf16[320,512]{1,0:T(8,128)(2,1)}, bf16[320,512]{1,0:T(8,128)(2,1)S(1)}, u32[]{:S(2)}, u32[]{:S(2)}) collective-permute-start(bf16[320,512]{1,0:T(8,128)(2,1)} %get-tuple-element.18), channel_id=1, source_target_pairs={{0,3},{1,0},{2,1},{3,2},{4,7},{5,4},{6,5},{7,6},{8,11},{9,8},{10,9... | collective-permute-start | bytes 983048 | tf_op jit(solution)/shard_map/ppermute | solution.py:434
  63.6 7.7 %collective-permute-done.1.refs_2_ = bf16[320,512]{1,0:T(8,128)(2,1)S(1)} collective-permute-done((bf16[320,512]{1,0:T(8,128)(2,1)}, bf16[320,512]{1,0:T(8,128)(2,1)S(1)}, u32[]{:S(2)}, u32[]{:S(2)}) %collective-permute-start.1) | collective-permute-done | bytes 327712 | tf_op jit(solution)/shard_map/ppermute | solution.py:434
  71.3 2.0 collective-permute-done.2.refs_3_
  74.4 4.7 %partial.1 = bf16[4,368,256]{2,1,0:T(8,128)(2,1)} custom-call(s32[2]{0:T(128)} %pad_add_fusion.side_ref, bf16[4,1280,128]{2,1,0:T(8,128)(2,1)} %copy-done.2, bf16[192,512]{1,0:T(8,128)(2,1)} %get-tuple-element.14.tokens_ref, bf16[320,512]{1,0:T(8,128)(2,1)} %get-tuple-element.15.refs_0_, bf16[320,512]{1,0:T(8,128)(2,1)} %copy-done.4, ...), custom_call_target="tpu_custom_call" | custom-call | tf_op jit(solution)/shard_map/partial/pallas_call | solution.py:323
  79.1 16.8 %all_to_all.31.parts_ref = bf16[4,368,256]{2,1,0:T(8,128)(2,1)} all-to-all(bf16[4,368,256]{2,1,0:T(8,128)(2,1)} %partial.1), channel_id=1, replica_groups={{0,1,2,3},{4,5,6,7},{8,9,10,11},{12,13,14,15},{16,17,18,19},{20,21,22,2..., dimensions={0} | all-to-all | bytes 1507328 | tf_op jit(solution)/shard_map/all_to_all | solution.py:28
  95.9 1.9 activate.1.refs_4_
  97.8 2.2 broadcast_in_dim.10
  100.0 6.9 %all-to-all-start.3 = ((bf16[16,368,128]{2,1,0:T(8,128)(2,1)}), bf16[16,368,128]{2,1,0:T(8,128)(2,1)S(1)}, u32[]{:S(2)}, u32[]{:S(2)}) async-start(bf16[16,368,128]{2,1,0:T(8,128)(2,1)} %broadcast_in_dim.10), calls=%async_computation.3 | async-start | bytes 3014656 | tf_op jit(solution)/shard_map/all_to_all | solution.py:28
  107.0 20.9 %all-to-all-done.3.hidden_ref = bf16[16,368,128]{2,1,0:T(8,128)(2,1)S(1)} async-done(((bf16[16,368,128]{2,1,0:T(8,128)(2,1)}), bf16[16,368,128]{2,1,0:T(8,128)(2,1)S(1)}, u32[]{:S(2)}, u32[]{:S(2)}) %all-to-all-start.3) | async-done | bytes 1507360 | tf_op jit(solution)/shard_map/all_to_all | solution.py:28
  129.0 3.9 %down.1 = (bf16[1280,128]{1,0:T(8,128)(2,1)}, f32[192,128]{1,0:T(8,128)}) custom-call(bf16[16,368,128]{2,1,0:T(8,128)(2,1)} %copy-done.1, bf16[4,512,128]{2,1,0:T(8,128)(2,1)} %w_ref.2, bf16[512,128]{1,0:T(8,128)(2,1)} %sw_ref.1), custom_call_target="tpu_custom_call" | custom-call | tf_op jit(solution)/shard_map/down/pallas_call | solution.py:368
  132.9 13.2 %all-to-all-start.5 = ((bf16[32,40,128]{2,1,0:T(8,128)(2,1)}), bf16[32,40,128]{2,1,0:T(8,128)(2,1)S(1)}, u32[]{:S(2)}, u32[]{:S(2)}) async-start(bf16[32,40,128]{2,1,0:T(8,128)(2,1)} %bitcast.22), calls=%async_computation.5 | async-start | bytes 655360 | tf_op jit(solution)/shard_map/all_to_all | solution.py:28
  146.2 38.7 %attention_first.1 = (f32[768,128]{1,0:T(8,128)}, f32[768,128]{1,0:T(8,128)}) custom-call(s32[1]{0:T(128)} %bitcast.ep_ref, bf16[64,768]{1,0:T(8,128)(2,1)} %bitcast.33, bf16[32,128,768]{2,1,0:T(8,128)(2,1)} %bitcast.31, f32[1,24576]{1,0:T(1,128)} %refs_3_.3, f32[1,24576]{1,0:T(1,128)} %refs_3_.3, bf16[368,128]{1,0:T(8,128)(2,1)} %activate.1.refs_4_), custom_call_target="tpu_custom_call" | custom-call | flops 9663676416 | bytes 4194304 | tf_op jit(solution)/shard_map/attention_first/pallas_call | solution.py:154
  184.9 28.0 %attention_rest.1 = bf16[384,128]{1,0:T(8,128)(2,1)} custom-call(s32[1]{0:T(128)} %bitcast.ep_ref, bf16[64,768]{1,0:T(8,128)(2,1)} %bitcast.34, bf16[32,128,768]{2,1,0:T(8,128)(2,1)} %bitcast.32, f32[1,24576]{1,0:T(1,128)} %refs_3_.3, f32[1,24576]{1,0:T(1,128)} %refs_3_.3, f32[768,128]{1,0:T(8,128)} %get-tuple-element.19.refs_4_, ...), custom_call_target="tpu_custom_call" | custom-call | flops 9663676416 | bytes 4194304 | tf_op jit(solution)/shard_map/attention_rest/pallas_call | solution.py:154
  212.8 2.5 broadcast_in_dim.11
  215.3 9.3 %all-to-all-start.4 = ((bf16[16,384,128]{2,1,0:T(8,128)(2,1)}), bf16[16,384,128]{2,1,0:T(8,128)(2,1)S(1)}, u32[]{:S(2)}, u32[]{:S(2)}) async-start(bf16[16,384,128]{2,1,0:T(8,128)(2,1)} %broadcast_in_dim.11), calls=%async_computation.4 | async-start | bytes 3145728 | tf_op jit(solution)/shard_map/all_to_all | solution.py:28
  224.6 2.6 combine.1
  227.2 24.4 %all-to-all-done.4.heads_ref = bf16[16,384,128]{2,1,0:T(8,128)(2,1)S(1)} async-done(((bf16[16,384,128]{2,1,0:T(8,128)(2,1)}), bf16[16,384,128]{2,1,0:T(8,128)(2,1)S(1)}, u32[]{:S(2)}, u32[]{:S(2)}) %all-to-all-start.4) | async-done | bytes 1572896 | tf_op jit(solution)/shard_map/all_to_all | solution.py:28
  252.8 3.1 %projection.1 = bf16[768,128]{1,0:T(8,128)(2,1)} custom-call(bf16[16,384,128]{2,1,0:T(8,128)(2,1)} %copy-done, bf16[1024,128]{1,0:T(8,128)(2,1)} %w_ref.3), custom_call_target="tpu_custom_call" | custom-call | flops 402653184 | bytes 4194304 | tf_op jit(solution)/shard_map/projection/pallas_call | solution.py:198
  (23 shorter events, 7.4 us)
Async XLA Ops:
  7.2 139.0 %all-gather.3.cloned.1.call-start = ((), (), s32[]{:S(2)}) async-start(), calls=%async_computation.6 | async-start | bytes 6488064 | tf_op jit(solution)/shard_map/all_gather | solution.py:424
  46.2 27.1 %all-to-all-start.1 = ((bf16[4,1280,128]{2,1,0:T(8,128)(2,1)}), bf16[4,1280,128]{2,1,0:T(8,128)(2,1)S(1)}, u32[]{:S(2)}, u32[]{:S(2)}) async-start(bf16[4,1280,128]{2,1,0:T(8,128)(2,1)} %broadcast_in_dim.9), calls=%async_computation.1 | async-start | bytes 2621440 | tf_op jit(solution)/shard_map/all_to_all | solution.py:28
  52.6 10.9 %collective-permute-start = (bf16[320,512]{1,0:T(8,128)(2,1)}, bf16[320,512]{1,0:T(8,128)(2,1)S(1)}, u32[]{:S(2)}, u32[]{:S(2)}) collective-permute-start(bf16[320,512]{1,0:T(8,128)(2,1)} %get-tuple-element.16), channel_id=1, source_target_pairs={{0,1},{1,2},{2,3},{3,0},{4,5},{5,6},{6,7},{7,4},{8,9},{9,10},{10,1... | collective-permute-start | bytes 983048 | tf_op jit(solution)/shard_map/ppermute | solution.py:434
  55.7 15.5 %collective-permute-start.1 = (bf16[320,512]{1,0:T(8,128)(2,1)}, bf16[320,512]{1,0:T(8,128)(2,1)S(1)}, u32[]{:S(2)}, u32[]{:S(2)}) collective-permute-start(bf16[320,512]{1,0:T(8,128)(2,1)} %get-tuple-element.17), channel_id=1, source_target_pairs={{0,2},{1,3},{2,0},{3,1},{4,6},{5,7},{6,4},{7,5},{8,10},{9,11},{10,... | collective-permute-start | bytes 983048 | tf_op jit(solution)/shard_map/ppermute | solution.py:434
  60.1 13.2 %collective-permute-start.2 = (bf16[320,512]{1,0:T(8,128)(2,1)}, bf16[320,512]{1,0:T(8,128)(2,1)S(1)}, u32[]{:S(2)}, u32[]{:S(2)}) collective-permute-start(bf16[320,512]{1,0:T(8,128)(2,1)} %get-tuple-element.18), channel_id=1, source_target_pairs={{0,3},{1,0},{2,1},{3,2},{4,7},{5,4},{6,5},{7,6},{8,11},{9,8},{10,9... | collective-permute-start | bytes 983048 | tf_op jit(solution)/shard_map/ppermute | solution.py:434
  63.6 9.7 %copy-start.4 = (bf16[320,512]{1,0:T(8,128)(2,1)}, bf16[320,512]{1,0:T(8,128)(2,1)S(1)}, u32[]{:S(2)}) copy-start(bf16[320,512]{1,0:T(8,128)(2,1)S(1)} %collective-permute-done.refs_1_) | copy-start | bytes 983044
  71.3 2.0 copy-start.5
  73.3 0.7 copy-start.6
  73.3 1.2 copy-start.2
  100.0 27.9 %all-to-all-start.3 = ((bf16[16,368,128]{2,1,0:T(8,128)(2,1)}), bf16[16,368,128]{2,1,0:T(8,128)(2,1)S(1)}, u32[]{:S(2)}, u32[]{:S(2)}) async-start(bf16[16,368,128]{2,1,0:T(8,128)(2,1)} %broadcast_in_dim.10), calls=%async_computation.3 | async-start | bytes 3014656 | tf_op jit(solution)/shard_map/all_to_all | solution.py:28
  127.9 1.1 copy-start.1
  132.9 79.9 %all-to-all-start.5 = ((bf16[32,40,128]{2,1,0:T(8,128)(2,1)}), bf16[32,40,128]{2,1,0:T(8,128)(2,1)S(1)}, u32[]{:S(2)}, u32[]{:S(2)}) async-start(bf16[32,40,128]{2,1,0:T(8,128)(2,1)} %bitcast.22), calls=%async_computation.5 | async-start | bytes 655360 | tf_op jit(solution)/shard_map/all_to_all | solution.py:28
  212.8 2.5 copy-start.3
  215.3 36.4 %all-to-all-start.4 = ((bf16[16,384,128]{2,1,0:T(8,128)(2,1)}), bf16[16,384,128]{2,1,0:T(8,128)(2,1)S(1)}, u32[]{:S(2)}, u32[]{:S(2)}) async-start(bf16[16,384,128]{2,1,0:T(8,128)(2,1)} %broadcast_in_dim.11), calls=%async_computation.4 | async-start | bytes 3145728 | tf_op jit(solution)/shard_map/all_to_all | solution.py:28
  251.6 1.2 copy-start
Sparse Core Ops, SparseCore 0:
  10.7 83.6 all-gather.2

commit v3 on v2

--- a/solution.py
+++ b/solution.py
@@ -39,6 +39,7 @@
 
 HEADROOM = 64.0
 EXTRA = 16
+GROUP = 2
 
 
 def three(x):
@@ -55,14 +56,16 @@
         q_ref, kv_ref, gk_ref, g0_ref, acc_in, m_in, _, out_ref, q_scr, m_scr, acc_scr = refs
     step = pl.program_id(0)
     own = ep_ref[0]
-    count = own // 2 if opening else own - own // 2
+    before = own // GROUP
+    count = before // 2 if opening else before - before // 2
     rows = q_scr.shape[0]
-    keys = kv_ref.shape[2]
+    keys = kv_ref.shape[2] * GROUP
 
     def operands():
-        kt = kv_ref[0, :HEAD, :]
+        kt = jnp.concatenate([kv_ref[n, :HEAD, :] for n in range(GROUP)], axis=1)
         row_id = lax.broadcasted_iota(jnp.int32, (2 * HEAD, keys), 0)
-        vt = jnp.where(row_id < HEAD, jnp.ones((), BF16), kv_ref[0])
+        both = jnp.concatenate([kv_ref[n] for n in range(GROUP)], axis=1)
+        vt = jnp.where(row_id < HEAD, jnp.ones((), BF16), both)
         gate = (gk_ref[...] - g0_ref[:, :1]) * LOG2E
         row_id = lax.broadcasted_iota(jnp.int32, (EXTRA, keys), 0)
         gates = jnp.zeros((EXTRA, keys), F32)
@@ -74,16 +77,15 @@
         kx, vt = operands()
         for i in range(rows // tile):
             span = pl.ds(i * tile, tile)
-            used = min(keys, (i + 1) * tile) if diagonal else keys
-            s = dot(q_scr[span, :], kx[:, :used])
+            s = dot(q_scr[span, :], kx)
             if diagonal:
-                q_pos = i * tile + lax.broadcasted_iota(jnp.int32, (tile, used), 0)
-                k_pos = lax.broadcasted_iota(jnp.int32, (tile, used), 1)
+                q_pos = own * rows + i * tile + lax.broadcasted_iota(jnp.int32, (tile, keys), 0)
+                k_pos = before * keys + lax.broadcasted_iota(jnp.int32, (tile, keys), 1)
                 s = jnp.where(k_pos <= q_pos, s, neg_fill)
             top = jnp.max(s, axis=1, keepdims=True)
             if diagonal:
                 p = jnp.exp2(s - top).astype(BF16)
-                acc_scr[target, span, :] = dot(p, vt[:, :used], NT)
+                acc_scr[target, span, :] = dot(p, vt, NT)
                 m_scr[span, :] = jnp.broadcast_to(top, (tile, m_scr.shape[1]))
             else:
                 old = m_scr[span, :]
@@ -132,46 +134,50 @@
             half = rows // 2
             top = acc_scr[last, :half, :]
             low = acc_scr[last, half:, :]
-            out_ref[...] = jnp.concatenate(
+            out = jnp.concatenate(
                 [top[:, HEAD:] / top[:, :HEAD], low[:, HEAD:] / low[:, :HEAD]], axis=1
             ).astype(BF16)
-
-
-def attention(ep_index, q_t, kv_all, cum_gate, state, after):
+            for n in range(out_ref.shape[0]):
+                out_ref[n] = out
+
+
+def attention(ep_index, q_t, kv_all, cum_gate, state, after, copies):
     blocks, wide, keys = kv_all.shape
     rows = q_t.shape[1]
     opening = state is None
+    steps = blocks // GROUP // 2
 
     def place(j, ep):
-        own = ep[0]
-        half = own // 2
+        before = ep[0] // GROUP
+        half = before // 2
         if opening:
-            return jnp.where(j == 0, own, jnp.maximum(jnp.minimum(j, half) - 1, 0))
-        return jnp.minimum(half + jnp.maximum(j - 1, 0), jnp.maximum(own - 1, 0))
+            return jnp.where(j == 0, before, jnp.maximum(jnp.minimum(j, half) - 1, 0))
+        return jnp.minimum(half + jnp.maximum(j - 1, 0), jnp.maximum(before - 1, 0))
 
     flat = pl.BlockSpec((rows, 128), lambda j, ep: (0, 0))
     wide_f32 = jax.ShapeDtypeStruct((rows, 128), F32)
+    sent = (copies, rows // 2, 2 * HEAD)
     return pl.pallas_call(
         functools.partial(attention_kernel, tile=384, opening=opening),
         grid_spec=pltpu.PrefetchScalarGridSpec(
             num_scalar_prefetch=1,
-            grid=(blocks // 2 + (0 if opening else 1),),
+            grid=(steps + (0 if opening else 1),),
             in_specs=[
                 pl.BlockSpec((HEAD, rows), lambda j, ep: (0, 0)),
-                pl.BlockSpec((1, wide, keys), lambda j, ep: (place(j, ep), 0, 0)),
-                pl.BlockSpec((1, keys), lambda j, ep: (0, place(j, ep))),
+                pl.BlockSpec((GROUP, wide, keys), lambda j, ep: (place(j, ep), 0, 0)),
+                pl.BlockSpec((1, GROUP * keys), lambda j, ep: (0, place(j, ep))),
                 pl.BlockSpec((1, keys), lambda j, ep: (0, ep[0])),
             ]
             + ([] if opening else [flat, flat])
             + [pl.BlockSpec(memory_space=pl.ANY)],
-            out_specs=(flat, flat) if opening else pl.BlockSpec((rows // 2, 2 * HEAD), lambda j, ep: (0, 0)),
+            out_specs=(flat, flat) if opening else pl.BlockSpec(sent, lambda j, ep: (0, 0, 0)),
             scratch_shapes=[
                 pltpu.VMEM((rows, 3 * HEAD + EXTRA), BF16),
                 pltpu.VMEM((rows, 128), F32),
                 pltpu.VMEM((2, rows, 128), F32),
             ],
         ),
-        out_shape=(wide_f32, wide_f32) if opening else jax.ShapeDtypeStruct((rows // 2, 2 * HEAD), BF16),
+        out_shape=(wide_f32, wide_f32) if opening else jax.ShapeDtypeStruct(sent, BF16),
         compiler_params=pltpu.CompilerParams(dimension_semantics=("arbitrary",)),
         cost_estimate=cost(2 * rows * keys * blocks * 256, 4 << 20),
         name="attention_first" if opening else "attention_rest",
@@ -203,44 +209,41 @@
     )(heads, out_weight)
 
 
-def spread_kernel(side_ref, gate_ref, up_ref, sg_ref, su_ref, *out_refs):
+def spread_kernel(tp_ref, gate_ref, up_ref, *out_refs):
     side = len(out_refs)
     experts, hidden, width = gate_ref.shape
     part = width // side
     block = experts * hidden
     for k, out_ref in enumerate(out_refs):
-        lanes = pl.ds(pl.multiple_of(lax.rem(side_ref[1] + k, side) * part, part), part)
+        lanes = pl.ds(pl.multiple_of(lax.rem(lax.rem(tp_ref[0], side) + k, side) * part, part), part)
         out_ref[:block, :] = gate_ref[:, :, lanes].reshape(block, part)
-        out_ref[block : 2 * block, :] = up_ref[:, :, lanes].reshape(block, part)
-        out_ref[2 * block : 2 * block + hidden, :] = sg_ref[:, lanes]
-        out_ref[2 * block + hidden :, :] = su_ref[:, lanes]
-
-
-def spread_weights(side_index, gate_t, up_t, sg_t, su_t, side):
+        out_ref[block:, :] = up_ref[:, :, lanes].reshape(block, part)
+
+
+def spread_weights(tp_index, gate_t, up_t, side):
     experts, hidden, width = gate_t.shape
     whole = pl.BlockSpec(memory_space=pltpu.VMEM)
-    rows = 2 * (experts + 1) * hidden
+    rows = 2 * experts * hidden
     return pl.pallas_call(
         spread_kernel,
-        in_specs=[pl.BlockSpec(memory_space=pltpu.SMEM)] + [whole] * 4,
+        in_specs=[pl.BlockSpec(memory_space=pltpu.SMEM)] + [whole] * 2,
         out_specs=[whole] * side,
         out_shape=[jax.ShapeDtypeStruct((rows, width // side), BF16)] * side,
         name="spread",
-    )(side_index, gate_t, up_t, sg_t, su_t)
+    )(tp_index, gate_t, up_t)
 
 
 def route_kernel(
-    side_ref, x_ref, gain_ref, routes_ref, weight_ref, slot_ref, mix_ref, part_ref, norm_scr,
+    tp_ref, x_ref, gain_ref, routes_ref, weight_ref, sg_ref, su_ref, slot_ref, mix_ref, shared_ref, norm_scr,
     *, side, groups, local_experts, room,
 ):
     tokens = x_ref.shape[0]
     x = x_ref[...].astype(F32)
     scale = lax.rsqrt(jnp.mean(x * x, axis=1, keepdims=True) + norm_eps)
-    norm_scr[...] = (x * scale * gain_ref[...]).astype(BF16)
+    normed = (x * scale * gain_ref[...]).astype(BF16)
+    norm_scr[...] = normed
     columns = slot_ref.shape[1]
-    wide = part_ref.shape[1]
-    part_ref[...] = norm_scr[:, pl.ds(pl.multiple_of(side_ref[1] * wide, wide), wide)]
-    start = pl.multiple_of((side_ref[1] * side + side_ref[0]) * columns, columns)
+    start = pl.multiple_of((lax.rem(tp_ref[0], side) * side + lax.div(tp_ref[0], side)) * columns, columns)
     piece = norm_scr[:, pl.ds(start, columns)]
     slots = groups * room
     shape = (groups, room, tokens)
@@ -264,24 +267,28 @@
     coarse = mix.astype(BF16)
     mix_ref[0] = coarse
     mix_ref[1] = (mix - coarse.astype(F32)).astype(BF16)
-
-
-def route(side_index, x, gain, routes_t, weight_t, side, groups, local_experts, room, columns):
+    gate_val = dot(normed, sg_ref[...], NT)
+    hidden = (gate_val / (1.0 + jnp.exp(-gate_val)) * dot(normed, su_ref[...], NT)).astype(BF16)
+    few = shared_ref.shape[0]
+    shared_ref[...] = jnp.concatenate([hidden[n * few : (n + 1) * few] for n in range(tokens // few)], axis=1)
+
+
+def route(tp_index, x, gain, routes_t, weight_t, sg_t, su_t, side, groups, local_experts, room, columns):
     tokens, width = x.shape
     slots = groups * room
     whole = pl.BlockSpec(memory_space=pltpu.VMEM)
     return pl.pallas_call(
         functools.partial(route_kernel, side=side, groups=groups, local_experts=local_experts, room=room),
-        in_specs=[pl.BlockSpec(memory_space=pltpu.SMEM)] + [whole] * 4,
+        in_specs=[pl.BlockSpec(memory_space=pltpu.SMEM)] + [whole] * 6,
         out_specs=(whole, whole, whole),
         out_shape=(
             jax.ShapeDtypeStruct((slots, columns), BF16),
             jax.ShapeDtypeStruct((2, slots, tokens), BF16),
-            jax.ShapeDtypeStruct((tokens, width // side), BF16),
+            jax.ShapeDtypeStruct((tokens * sg_t.shape[0] // columns, columns), BF16),
         ),
         scratch_shapes=[pltpu.VMEM((tokens, width), BF16)],
         name="route",
-    )(side_index, x, gain, routes_t, weight_t)
+    )(tp_index, x, gain, routes_t, weight_t, sg_t, su_t)
 
 
 def by_expert(rows, count):
@@ -289,13 +296,13 @@
     return jnp.concatenate([jnp.where(own == e, rows, jnp.zeros((), rows.dtype)) for e in range(count)], axis=1)
 
 
-def partial_kernel(side_ref, rows_ref, tokens_ref, *refs, count, hidden):
-    side = len(refs) - 3
-    out_ref, w_scr, shared_scr = refs[side:]
+def partial_kernel(tp_ref, rows_ref, *refs, count, hidden):
+    side = len(refs) - 2
+    out_ref, w_scr = refs[side:]
     wide = side * hidden
     depth = rows_ref.shape[2]
     for k in range(side):
-        place = pl.multiple_of(lax.rem(side_ref[1] + side - k, side) * hidden, hidden)
+        place = pl.multiple_of(lax.rem(lax.rem(tp_ref[0], side) + side - k, side) * hidden, hidden)
         for g in range(2):
             span = pl.ds(g * wide + place, hidden)
             for e in range(count):
@@ -303,66 +310,65 @@
                 for c in range(side):
                     lanes = (c * count + e) * depth
                     w_scr[span, lanes : lanes + depth] = refs[k][first : first + hidden, c * depth : (c + 1) * depth]
-            first = (2 * count + g) * hidden
-            shared_scr[span, :] = refs[k][first : first + hidden, :]
-    each = rows_ref.shape[1] // side
-    few = tokens_ref.shape[0] // side
+    each = out_ref.shape[1]
     for n in range(side):
         total = jnp.zeros((each, 2 * wide), F32)
         for c in range(side):
             spread = by_expert(rows_ref[c, n * each : (n + 1) * each, :], count)
             total = total + dot(spread, w_scr[:, c * count * depth : (c + 1) * count * depth], NT)
-        out_ref[n, :each, :] = total.astype(BF16)
-        out_ref[n, each:, :] = dot(tokens_ref[n * few : (n + 1) * few, :], shared_scr[...], NT).astype(BF16)
-
-
-def partial_products(side_index, rows, tokens, weights, count, hidden):
+        out_ref[n] = total.astype(BF16)
+
+
+def partial_products(tp_index, rows, weights, count, hidden):
     side = len(weights)
     whole = pl.BlockSpec(memory_space=pltpu.VMEM)
-    each = (rows.shape[1] + tokens.shape[0]) // side
     return pl.pallas_call(
         functools.partial(partial_kernel, count=count, hidden=hidden),
-        in_specs=[pl.BlockSpec(memory_space=pltpu.SMEM)] + [whole] * (2 + side),
+        in_specs=[pl.BlockSpec(memory_space=pltpu.SMEM)] + [whole] * (1 + side),
         out_specs=whole,
-        out_shape=jax.ShapeDtypeStruct((side, each, 2 * side * hidden), BF16),
-        scratch_shapes=[
-            pltpu.VMEM((2 * side * hidden, count * side * rows.shape[2]), BF16),
-            pltpu.VMEM((2 * side * hidden, tokens.shape[1]), BF16),
-        ],
+        out_shape=jax.ShapeDtypeStruct((side, rows.shape[1] // side, 2 * side * hidden), BF16),
+        scratch_shapes=[pltpu.VMEM((2 * side * hidden, count * side * rows.shape[2]), BF16)],
         name="partial",
-    )(side_index, rows, tokens, *weights)
-
-
-def activate_kernel(parts_ref, out_ref):
+    )(tp_index, rows, *weights)
+
+
+def activate_kernel(parts_ref, shared_ref, out_ref):
     total = parts_ref[0].astype(F32)
     for t in range(1, parts_ref.shape[0]):
         total = total + parts_ref[t].astype(F32)
-    half = out_ref.shape[1]
+    rows, half = total.shape[0], out_ref.shape[2]
     gate_val = total[:, :half]
-    out_ref[...] = (gate_val / (1.0 + jnp.exp(-gate_val)) * total[:, half:]).astype(BF16)
-
-
-def activate(parts):
+    hidden = (gate_val / (1.0 + jnp.exp(-gate_val)) * total[:, half:]).astype(BF16)
+    for n in range(out_ref.shape[0]):
+        out_ref[n, :rows, :] = hidden
+        out_ref[n, rows:, :] = shared_ref[...]
+
+
+def activate(parts, shared, copies):
     _, rows, width = parts.shape
     return pl.pallas_call(
         activate_kernel,
-        out_shape=jax.ShapeDtypeStruct((rows, width // 2), BF16),
+        out_shape=jax.ShapeDtypeStruct((copies, rows + shared.shape[0], width // 2), BF16),
         name="activate",
-    )(parts)
+    )(parts, shared)
 
 
 def down_kernel(hidden_ref, w_ref, sw_ref, out_ref, shared_ref, *, side):
     count, hidden, columns = w_ref.shape
+    peers = hidden_ref.shape[0]
     each = out_ref.shape[0] // side
-    few = shared_ref.shape[0] // side
     w = w_ref[...].reshape(count * hidden, columns)
     for n in range(side):
-        rows = jnp.concatenate([hidden_ref[y * side + n] for y in range(side)], axis=1)
-        out_ref[n * each : (n + 1) * each, :] = dot(by_expert(rows[:each], count), w).astype(BF16)
-        shared_ref[n * few : (n + 1) * few, :] = dot(rows[each:], sw_ref[...])
-
-
-def down(hidden, weights, shared_down, side, slots):
+        rows = jnp.concatenate([hidden_ref[y * side + n, :each, :] for y in range(side)], axis=1)
+        out_ref[n * each : (n + 1) * each, :] = dot(by_expert(rows, count), w).astype(BF16)
+    few = hidden_ref.shape[1] - each
+    units = sw_ref.shape[0] // peers
+    for n in range(shared_ref.shape[0] // few):
+        rows = jnp.concatenate([hidden_ref[t, each:, n * units : (n + 1) * units] for t in range(peers)], axis=1)
+        shared_ref[n * few : (n + 1) * few, :] = dot(rows, sw_ref[...])
+
+
+def down(hidden, weights, shared_down, side, slots, tokens):
     columns = weights.shape[2]
     whole = pl.BlockSpec(memory_space=pltpu.VMEM)
     return pl.pallas_call(
@@ -371,7 +377,7 @@
         out_specs=(whole, whole),
         out_shape=(
             jax.ShapeDtypeStruct((slots, columns), BF16),
-            jax.ShapeDtypeStruct((hidden.shape[1] * side - slots, columns), F32),
+            jax.ShapeDtypeStruct((tokens, columns), F32),
         ),
         name="down",
     )(hidden, weights, shared_down)
@@ -414,38 +420,33 @@
     along_x = [[y * side + x for x in range(side)] for y in range(side)]
     along_y = [[y * side + x for y in range(side)] for x in range(side)]
     ep_index = lax.axis_index("ep").astype(jnp.int32).reshape(1)
-    tp_index = lax.axis_index("tp").astype(jnp.int32)
-    side_index = jnp.stack([tp_index // side, tp_index % side])
+    tp_index = lax.axis_index("tp").astype(jnp.int32).reshape(1)
     local_experts, _, hidden_each = expert_gate.shape
     columns = expert_down.shape[2]
     room = -(-CAP * local_experts // 8) * 8
     slot_count = groups * room
     key_value = jnp.concatenate([key_rows.T, value_rows.T], axis=0)
     kv_all = lax.all_gather(key_value, "ep", axis=0)
-    slots, mix, tokens = route(
-        side_index, moe_input, moe_gain.reshape(1, -1), routes.T, route_weight.T,
+    slots, mix, shared = route(
+        tp_index, moe_input, moe_gain.reshape(1, -1), routes.T, route_weight.T, shared_gate.T, shared_up.T,
         side, groups, local_experts, room, columns,
     )
     arrived = exchanged(slots.reshape(groups, room, columns), "ep")
-    pieces = spread_weights(
-        side_index, expert_gate.transpose(0, 2, 1), expert_up.transpose(0, 2, 1), shared_gate.T, shared_up.T, side
-    )
-    pieces = [pieces[0]] + [
-        lax.ppermute(
-            pieces[k], "tp", [(row[x], row[(x + k) % side]) for row in along_x for x in range(side)]
-        )
-        for k in range(1, side)
-    ]
+    pieces = spread_weights(tp_index, expert_gate.transpose(0, 2, 1), expert_up.transpose(0, 2, 1), side)
+    pieces = list(pieces)
+    for k in sorted(range(1, side), key=lambda k: -min(k, side - k)):
+        steps = [(row[x], row[(x + k) % side]) for row in along_x for x in range(side)]
+        pieces[k] = lax.ppermute(pieces[k], "tp", steps)
     gathered = sent_to_all(arrived.reshape(slot_count, columns), "tp", along_y)
-    parts = partial_products(side_index, gathered, tokens, pieces, local_experts, hidden_each)
+    parts = partial_products(tp_index, gathered, pieces, local_experts, hidden_each)
     parts = exchanged(parts, "tp", along_x)
-    own_hidden = activate(parts)
-    hidden = sent_to_all(own_hidden, "tp")
-    state = attention(ep_index, query_rows.T, kv_all, cum_gate, None, own_hidden)
-    result, shared = down(hidden, expert_down, shared_down, side, slot_count)
+    own_hidden = activate(parts, shared, peers)
+    hidden = exchanged(own_hidden, "tp")
+    state = attention(ep_index, query_rows.T, kv_all, cum_gate, None, own_hidden, peers)
+    result, shared = down(hidden, expert_down, shared_down, side, slot_count, moe_input.shape[0])
     back = exchanged(result.reshape(groups, room, columns), "ep")
-    heads = attention(ep_index, query_rows.T, kv_all, cum_gate, state, result)
-    heads = sent_to_all(heads, "tp")
+    heads = attention(ep_index, query_rows.T, kv_all, cum_gate, state, result, peers)
+    heads = exchanged(heads, "tp")
     mixer_out = projection(heads, out_weight)
     moe_out = combine(mix, back.reshape(slot_count, columns), shared)
     return (mixer_out, moe_out)

time: 264 us -> 242 us (0.917)
  waiting for transfers between devices: 55.5 us -> 48.5 us
  Pallas kernels: 89.4 us -> 84.2 us
  local copies, waits for them, and re-layouts: 9.32 us -> 5.5 us
  starting transfers between devices: 44 us -> 40.9 us
    pallas_call x2, Pallas kernels: 66.6 us -> 61.6 us  [attention(): pl.pallas_call(functools.partial(attention_kernel, tile=384, opening=open...]
    broadcast_in_dim x3 -> x1, local copies, waits for them, and re-layouts: 5.89 us -> 1.22 us  [sent_to_all(): jnp.broadcast_to(array, (count, *array.shape))]
    all_to_all x4, waiting for transfers between devices: 45.4 us -> 41 us  [exchanged(): lax.all_to_all(array, axis, split_axis=0, concat_axis=0, tiled=True, axis...]
    all_to_all x4, starting transfers between devices: 33.5 us -> 30.4 us  [exchanged(): lax.all_to_all(array, axis, split_axis=0, concat_axis=0, tiled=True, axis...]
    ppermute x3, waiting for transfers between devices: 10.1 us -> 7.45 us  [local(): pieces[k] = lax.ppermute(pieces[k], 'tp', steps)]
  transfers between devices with their start and end apart: 8 -> 8, of which waited for: 5 -> 4; matrix products, arithmetic and copies ran while one was open for 2% -> 1% of each run, Pallas kernels for 33% -> 34%
where the time goes in v3:
time: 242 us; the launch traced here: 241 us
  Pallas kernels  84.2 us (35%)
  waiting for transfers between devices  48.5 us (20%)
  blocking collectives  46.3 us (19%)
  starting transfers between devices  40.9 us (17%)
  between operations  14.1 us (6%)
  local copies, waits for them, and re-layouts  5.5 us (2%)
    pallas_call x2, Pallas kernels, attention(): pl.pallas_call(functools.partial(attention_kernel, tile=384, opening=open...  61.6 us
    all_to_all x2, blocking collectives, exchanged(): lax.all_to_all(array, axis, split_axis=0, concat_axis=0, tiled=True, axis...  46.3 us
    all_to_all x4, waiting for transfers between devices, exchanged(): lax.all_to_all(array, axis, split_axis=0, concat_axis=0, tiled=True, axis...  41 us
    all_to_all x4, starting transfers between devices, exchanged(): lax.all_to_all(array, axis, split_axis=0, concat_axis=0, tiled=True, axis...  30.4 us
    ppermute x3, starting transfers between devices, local(): pieces[k] = lax.ppermute(pieces[k], 'tp', steps)  10.5 us
    ppermute x3, waiting for transfers between devices, local(): pieces[k] = lax.ppermute(pieces[k], 'tp', steps)  7.45 us
  transfers between devices with their start and end apart: 8, of which 4 were waited for; matrix products, arithmetic and copies ran while one was open for 1% of the time, Pallas kernels for 34%

profile of v3, /device:TPU:481, one launch (start us, length us, event | category | flops | bytes accessed | tf_op | source)
XLA Modules:
  0.0 241.3 jit_solution(12808856083287964392)
XLA Ops:
  7.2 1.6 pad_maximum_fusion
  8.9 4.2 %route.1 = (bf16[1280,128]{1,0:T(8,128)(2,1)}, bf16[2,1280,192]{2,1,0:T(8,128)(2,1)}, bf16[48,128]{1,0:T(8,128)(2,1)}) custom-call(s32[1]{0:T(128)} %bitcast.5.tp_ref, bf16[192,2048]{1,0:T(8,128)(2,1)} %x_ref.1, f32[1,2048]{1,0:T(1,128)} %bitcast.27, s32[3,192]{1,0:T(4,128)} %bitcast.28, f32[3,192]{1,0:T(4,128)} %bitcast.29, bf16[32,2048]{1,0:T(8,128)(2,1)} %bitcast.23, ...), custom_call_target="tpu_custom_call" | custom-call | tf_op jit(solution)/shard_map/route/pallas_call | solution.py:280
  13.1 31.0 %all_to_all.30 = bf16[32,40,128]{2,1,0:T(8,128)(2,1)S(1)} all-to-all(bf16[32,40,128]{2,1,0:T(8,128)(2,1)} %bitcast.22), channel_id=1, replica_groups=mesh['ep'=32,'tp'=16] {'ep'}, dimensions={0} | all-to-all | bytes 655360 | tf_op jit(solution)/shard_map/all_to_all | solution.py:28
  44.1 1.2 broadcast_in_dim.3
  45.3 4.3 %all-to-all-start.1 = ((bf16[4,1280,128]{2,1,0:T(8,128)(2,1)}), bf16[4,1280,128]{2,1,0:T(8,128)(2,1)S(1)}, u32[]{:S(2)}, u32[]{:S(2)}) async-start(bf16[4,1280,128]{2,1,0:T(8,128)(2,1)} %broadcast_in_dim.3), calls=%async_computation.1 | async-start | bytes 2621440 | tf_op jit(solution)/shard_map/all_to_all | solution.py:28
  49.6 2.3 spread.1
  51.9 3.1 %collective-permute-start = (bf16[256,512]{1,0:T(8,128)(2,1)}, bf16[256,512]{1,0:T(8,128)(2,1)S(1)}, u32[]{:S(2)}, u32[]{:S(2)}) collective-permute-start(bf16[256,512]{1,0:T(8,128)(2,1)} %get-tuple-element.15), channel_id=1, source_target_pairs={{0,1},{1,2},{2,3},{3,0},{4,5},{5,6},{6,7},{7,4},{8,9},{9,10},{10,1... | collective-permute-start | bytes 786440 | tf_op jit(solution)/shard_map/ppermute | solution.py:439
  55.0 4.4 %collective-permute-start.1 = (bf16[256,512]{1,0:T(8,128)(2,1)}, bf16[256,512]{1,0:T(8,128)(2,1)S(1)}, u32[]{:S(2)}, u32[]{:S(2)}) collective-permute-start(bf16[256,512]{1,0:T(8,128)(2,1)} %get-tuple-element.16), channel_id=1, source_target_pairs={{0,2},{1,3},{2,0},{3,1},{4,6},{5,7},{6,4},{7,5},{8,10},{9,11},{10,... | collective-permute-start | bytes 786440 | tf_op jit(solution)/shard_map/ppermute | solution.py:439
  59.4 3.1 %collective-permute-start.2 = (bf16[256,512]{1,0:T(8,128)(2,1)}, bf16[256,512]{1,0:T(8,128)(2,1)S(1)}, u32[]{:S(2)}, u32[]{:S(2)}) collective-permute-start(bf16[256,512]{1,0:T(8,128)(2,1)} %get-tuple-element.17), channel_id=1, source_target_pairs={{0,3},{1,0},{2,1},{3,2},{4,7},{5,4},{6,5},{7,6},{8,11},{9,8},{10,9... | collective-permute-start | bytes 786440 | tf_op jit(solution)/shard_map/ppermute | solution.py:439
  62.5 6.0 %collective-permute-done.1.refs_2_ = bf16[256,512]{1,0:T(8,128)(2,1)S(1)} collective-permute-done((bf16[256,512]{1,0:T(8,128)(2,1)}, bf16[256,512]{1,0:T(8,128)(2,1)S(1)}, u32[]{:S(2)}, u32[]{:S(2)}) %collective-permute-start.1) | collective-permute-done | bytes 262176 | tf_op jit(solution)/shard_map/ppermute | solution.py:439
  68.5 1.4 collective-permute-done.2.refs_3_
  71.1 4.2 %partial.1 = bf16[4,320,256]{2,1,0:T(8,128)(2,1)} custom-call(s32[1]{0:T(128)} %bitcast.5.tp_ref, bf16[4,1280,128]{2,1,0:T(8,128)(2,1)} %copy-done.2, bf16[256,512]{1,0:T(8,128)(2,1)} %get-tuple-element.14.refs_0_, bf16[256,512]{1,0:T(8,128)(2,1)} %copy-done.4, bf16[256,512]{1,0:T(8,128)(2,1)} %copy-done.5, bf16[256,512]{1,0:T(8,128)(2,1)} %copy-done.6), custom_call_target="tpu_custom_call" | custom-call | tf_op jit(solution)/shard_map/partial/pallas_call | solution.py:325
  75.3 15.4 %all_to_all.31.parts_ref = bf16[4,320,256]{2,1,0:T(8,128)(2,1)} all-to-all(bf16[4,320,256]{2,1,0:T(8,128)(2,1)} %partial.1), channel_id=1, replica_groups={{0,1,2,3},{4,5,6,7},{8,9,10,11},{12,13,14,15},{16,17,18,19},{20,21,22,2..., dimensions={0} | all-to-all | bytes 1310720 | tf_op jit(solution)/shard_map/all_to_all | solution.py:28
  90.7 2.4 activate.1.refs_4_
  93.0 6.9 %all-to-all-start.3 = ((bf16[16,368,128]{2,1,0:T(8,128)(2,1)}), bf16[16,368,128]{2,1,0:T(8,128)(2,1)S(1)}, u32[]{:S(2)}, u32[]{:S(2)}) async-start(bf16[16,368,128]{2,1,0:T(8,128)(2,1)} %activate.1.refs_4_), calls=%async_computation.3 | async-start | bytes 3014656 | tf_op jit(solution)/shard_map/all_to_all | solution.py:28
  99.9 20.5 %all-to-all-done.3.hidden_ref = bf16[16,368,128]{2,1,0:T(8,128)(2,1)S(1)} async-done(((bf16[16,368,128]{2,1,0:T(8,128)(2,1)}), bf16[16,368,128]{2,1,0:T(8,128)(2,1)S(1)}, u32[]{:S(2)}, u32[]{:S(2)}) %all-to-all-start.3) | async-done | bytes 1507360 | tf_op jit(solution)/shard_map/all_to_all | solution.py:28
  121.6 3.9 %down.1 = (bf16[1280,128]{1,0:T(8,128)(2,1)}, f32[192,128]{1,0:T(8,128)}) custom-call(bf16[16,368,128]{2,1,0:T(8,128)(2,1)} %copy-done.1, bf16[4,512,128]{2,1,0:T(8,128)(2,1)} %w_ref.2, bf16[512,128]{1,0:T(8,128)(2,1)} %sw_ref.1), custom_call_target="tpu_custom_call" | custom-call | tf_op jit(solution)/shard_map/down/pallas_call | solution.py:374
  125.5 13.1 %all-to-all-start.5 = ((bf16[32,40,128]{2,1,0:T(8,128)(2,1)}), bf16[32,40,128]{2,1,0:T(8,128)(2,1)S(1)}, u32[]{:S(2)}, u32[]{:S(2)}) async-start(bf16[32,40,128]{2,1,0:T(8,128)(2,1)} %bitcast.21), calls=%async_computation.5 | async-start | bytes 655360 | tf_op jit(solution)/shard_map/all_to_all | solution.py:28
  138.6 33.3 %attention_first.1 = (f32[768,128]{1,0:T(8,128)}, f32[768,128]{1,0:T(8,128)}) custom-call(s32[1]{0:T(128)} %bitcast.ep_ref, bf16[64,768]{1,0:T(8,128)(2,1)} %bitcast.32, bf16[32,128,768]{2,1,0:T(8,128)(2,1)} %bitcast.30, f32[1,24576]{1,0:T(1,128)} %refs_3_.3, f32[1,24576]{1,0:T(1,128)} %refs_3_.3, bf16[16,368,128]{2,1,0:T(8,128)(2,1)} %activate.1.refs_4_), custom_call_target="tpu_custom_call" | custom-call | flops 9663676416 | bytes 4194304 | tf_op jit(solution)/shard_map/attention_first/pallas_call | solution.py:160
  171.8 28.3 %attention_rest.1 = bf16[16,384,128]{2,1,0:T(8,128)(2,1)} custom-call(s32[1]{0:T(128)} %bitcast.ep_ref, bf16[64,768]{1,0:T(8,128)(2,1)} %bitcast.33, bf16[32,128,768]{2,1,0:T(8,128)(2,1)} %bitcast.31, f32[1,24576]{1,0:T(1,128)} %refs_3_.3, f32[1,24576]{1,0:T(1,128)} %refs_3_.3, f32[768,128]{1,0:T(8,128)} %get-tuple-element.19.refs_4_, ...), custom_call_target="tpu_custom_call" | custom-call | flops 9663676416 | bytes 4194304 | tf_op jit(solution)/shard_map/attention_rest/pallas_call | solution.py:160
  200.9 6.1 %all-to-all-start.4 = ((bf16[16,384,128]{2,1,0:T(8,128)(2,1)}), bf16[16,384,128]{2,1,0:T(8,128)(2,1)S(1)}, u32[]{:S(2)}, u32[]{:S(2)}) async-start(bf16[16,384,128]{2,1,0:T(8,128)(2,1)} %attention_rest.1), calls=%async_computation.4 | async-start | bytes 3145728 | tf_op jit(solution)/shard_map/all_to_all | solution.py:28
  207.1 2.6 %combine.1 = bf16[192,128]{1,0:T(8,128)(2,1)} custom-call(bf16[2,1280,192]{2,1,0:T(8,128)(2,1)} %get-tuple-element.22.mix_ref, bf16[1280,128]{1,0:T(8,128)(2,1)} %bitcast.17, f32[192,128]{1,0:T(8,128)} %get-tuple-element.23.shared_ref), custom_call_target="tpu_custom_call" | custom-call | tf_op jit(solution)/shard_map/combine/pallas_call | solution.py:393
  209.7 20.5 %all-to-all-done.4.heads_ref = bf16[16,384,128]{2,1,0:T(8,128)(2,1)S(1)} async-done(((bf16[16,384,128]{2,1,0:T(8,128)(2,1)}), bf16[16,384,128]{2,1,0:T(8,128)(2,1)S(1)}, u32[]{:S(2)}, u32[]{:S(2)}) %all-to-all-start.4) | async-done | bytes 1572896 | tf_op jit(solution)/shard_map/all_to_all | solution.py:28
  231.4 3.1 %projection.1 = bf16[768,128]{1,0:T(8,128)(2,1)} custom-call(bf16[16,384,128]{2,1,0:T(8,128)(2,1)} %copy-done, bf16[1024,128]{1,0:T(8,128)(2,1)} %w_ref.3), custom_call_target="tpu_custom_call" | custom-call | flops 402653184 | bytes 4194304 | tf_op jit(solution)/shard_map/projection/pallas_call | solution.py:204
  (20 shorter events, 4.4 us)
Async XLA Ops:
  7.2 131.4 %all-gather.3.cloned.1.call-start = ((), (), s32[]{:S(2)}) async-start(), calls=%async_computation.6 | async-start | bytes 6488064 | tf_op jit(solution)/shard_map/all_gather | solution.py:429
  45.3 24.6 %all-to-all-start.1 = ((bf16[4,1280,128]{2,1,0:T(8,128)(2,1)}), bf16[4,1280,128]{2,1,0:T(8,128)(2,1)S(1)}, u32[]{:S(2)}, u32[]{:S(2)}) async-start(bf16[4,1280,128]{2,1,0:T(8,128)(2,1)} %broadcast_in_dim.3), calls=%async_computation.1 | async-start | bytes 2621440 | tf_op jit(solution)/shard_map/all_to_all | solution.py:28
  51.9 10.5 %collective-permute-start = (bf16[256,512]{1,0:T(8,128)(2,1)}, bf16[256,512]{1,0:T(8,128)(2,1)S(1)}, u32[]{:S(2)}, u32[]{:S(2)}) collective-permute-start(bf16[256,512]{1,0:T(8,128)(2,1)} %get-tuple-element.15), channel_id=1, source_target_pairs={{0,1},{1,2},{2,3},{3,0},{4,5},{5,6},{6,7},{7,4},{8,9},{9,10},{10,1... | collective-permute-start | bytes 786440 | tf_op jit(solution)/shard_map/ppermute | solution.py:439
  55.0 13.5 %collective-permute-start.1 = (bf16[256,512]{1,0:T(8,128)(2,1)}, bf16[256,512]{1,0:T(8,128)(2,1)S(1)}, u32[]{:S(2)}, u32[]{:S(2)}) collective-permute-start(bf16[256,512]{1,0:T(8,128)(2,1)} %get-tuple-element.16), channel_id=1, source_target_pairs={{0,2},{1,3},{2,0},{3,1},{4,6},{5,7},{6,4},{7,5},{8,10},{9,11},{10,... | collective-permute-start | bytes 786440 | tf_op jit(solution)/shard_map/ppermute | solution.py:439
  59.4 10.5 %collective-permute-start.2 = (bf16[256,512]{1,0:T(8,128)(2,1)}, bf16[256,512]{1,0:T(8,128)(2,1)S(1)}, u32[]{:S(2)}, u32[]{:S(2)}) collective-permute-start(bf16[256,512]{1,0:T(8,128)(2,1)} %get-tuple-element.17), channel_id=1, source_target_pairs={{0,3},{1,0},{2,1},{3,2},{4,7},{5,4},{6,5},{7,6},{8,11},{9,8},{10,9... | collective-permute-start | bytes 786440 | tf_op jit(solution)/shard_map/ppermute | solution.py:439
  62.5 7.5 %copy-start.4 = (bf16[256,512]{1,0:T(8,128)(2,1)}, bf16[256,512]{1,0:T(8,128)(2,1)S(1)}, u32[]{:S(2)}) copy-start(bf16[256,512]{1,0:T(8,128)(2,1)S(1)} %collective-permute-done.refs_1_) | copy-start | bytes 786436
  68.5 1.4 copy-start.5
  69.9 0.7 copy-start.6
  69.9 1.1 copy-start.2
  93.0 27.3 %all-to-all-start.3 = ((bf16[16,368,128]{2,1,0:T(8,128)(2,1)}), bf16[16,368,128]{2,1,0:T(8,128)(2,1)S(1)}, u32[]{:S(2)}, u32[]{:S(2)}) async-start(bf16[16,368,128]{2,1,0:T(8,128)(2,1)} %activate.1.refs_4_), calls=%async_computation.3 | async-start | bytes 3014656 | tf_op jit(solution)/shard_map/all_to_all | solution.py:28
  120.4 1.2 copy-start.1
  125.5 74.7 %all-to-all-start.5 = ((bf16[32,40,128]{2,1,0:T(8,128)(2,1)}), bf16[32,40,128]{2,1,0:T(8,128)(2,1)S(1)}, u32[]{:S(2)}, u32[]{:S(2)}) async-start(bf16[32,40,128]{2,1,0:T(8,128)(2,1)} %bitcast.21), calls=%async_computation.5 | async-start | bytes 655360 | tf_op jit(solution)/shard_map/all_to_all | solution.py:28
  200.2 0.8 copy-start.3
  200.9 29.2 %all-to-all-start.4 = ((bf16[16,384,128]{2,1,0:T(8,128)(2,1)}), bf16[16,384,128]{2,1,0:T(8,128)(2,1)S(1)}, u32[]{:S(2)}, u32[]{:S(2)}) async-start(bf16[16,384,128]{2,1,0:T(8,128)(2,1)} %attention_rest.1), calls=%async_computation.4 | async-start | bytes 3145728 | tf_op jit(solution)/shard_map/all_to_all | solution.py:28
  230.2 1.2 copy-start
Sparse Core Ops, SparseCore 0:
  10.7 83.0 all-gather.2

commit v4 on v3

--- a/solution.py
+++ b/solution.py
@@ -26,11 +26,6 @@
 
 def exchanged(array, axis, among=None):
     return lax.all_to_all(array, axis, split_axis=0, concat_axis=0, tiled=True, axis_index_groups=among)
-
-
-def sent_to_all(array, axis, among=None):
-    count = len(among[0]) if among else lax.axis_size(axis)
-    return exchanged(jnp.broadcast_to(array, (count, *array.shape)), axis, among)
 
 
 def cost(flops, nbytes):
@@ -186,16 +181,18 @@
 
 def projection_kernel(heads_ref, w_ref, out_ref):
     count, half, _ = heads_ref.shape
-    acc = jnp.zeros((half, 2 * w_ref.shape[1]), F32)
-    blank = jnp.zeros((HEAD, w_ref.shape[1]), BF16)
-    for h in range(count):
-        w = w_ref[h * HEAD : (h + 1) * HEAD, :]
-        both = jnp.concatenate(
-            [jnp.concatenate([w, blank], axis=1), jnp.concatenate([blank, w], axis=1)], axis=0
-        )
-        acc = acc + dot(heads_ref[h], both)
-    out_ref[:half, :] = acc[:, : w_ref.shape[1]].astype(BF16)
-    out_ref[half:, :] = acc[:, w_ref.shape[1] :].astype(BF16)
+    columns = w_ref.shape[1]
+    blank = jnp.zeros((HEAD, columns), BF16)
+    acc = jnp.zeros((half, 2 * columns), F32)
+    for h in range(0, count, 2):
+        both = []
+        for n in range(h, h + 2):
+            w = w_ref[n * HEAD : (n + 1) * HEAD, :]
+            both += [jnp.concatenate([w, blank], axis=1), jnp.concatenate([blank, w], axis=1)]
+        rows = jnp.concatenate([heads_ref[h], heads_ref[h + 1]], axis=1)
+        acc = acc + dot(rows, jnp.concatenate(both, axis=0))
+    out_ref[:half, :] = acc[:, :columns].astype(BF16)
+    out_ref[half:, :] = acc[:, columns:].astype(BF16)
 
 
 def projection(heads, out_weight):
@@ -233,67 +230,98 @@
     )(tp_index, gate_t, up_t)
 
 
-def route_kernel(
-    tp_ref, x_ref, gain_ref, routes_ref, weight_ref, sg_ref, su_ref, slot_ref, mix_ref, shared_ref, norm_scr,
-    *, side, groups, local_experts, room,
-):
-    tokens = x_ref.shape[0]
+def normed_rows(x_ref, gain_ref):
     x = x_ref[...].astype(F32)
     scale = lax.rsqrt(jnp.mean(x * x, axis=1, keepdims=True) + norm_eps)
-    normed = (x * scale * gain_ref[...]).astype(BF16)
-    norm_scr[...] = normed
-    columns = slot_ref.shape[1]
-    start = pl.multiple_of((lax.rem(tp_ref[0], side) * side + lax.div(tp_ref[0], side)) * columns, columns)
-    piece = norm_scr[:, pl.ds(start, columns)]
-    slots = groups * room
+    return (x * scale * gain_ref[...]).astype(BF16)
+
+
+def slot_choice(routes_ref, groups, local_experts, room):
+    tokens = routes_ref.shape[1]
     shape = (groups, room, tokens)
     within = lax.broadcasted_iota(jnp.int32, shape, 1)
     expert = lax.broadcasted_iota(jnp.int32, shape, 0) * local_experts + within % local_experts
-    expert = expert.reshape(slots, tokens)
-    turn = (within // local_experts).reshape(slots, tokens).astype(F32)
-    hit = jnp.zeros((slots, tokens), F32)
-    weight = jnp.zeros((slots, tokens), F32)
-    for j in range(routes_ref.shape[0]):
-        same = expert == routes_ref[j : j + 1, :]
-        hit = hit + jnp.where(same, 1.0, 0.0)
-        weight = weight + jnp.where(same, weight_ref[j : j + 1, :], 0.0)
+    expert = expert.reshape(groups * room, tokens)
+    turn = (within // local_experts).reshape(groups * room, tokens).astype(F32)
+    same = [expert == routes_ref[j : j + 1, :] for j in range(routes_ref.shape[0])]
+    hit = sum(jnp.where(one, 1.0, 0.0) for one in same)
     before = lax.broadcasted_iota(jnp.int32, (tokens, tokens), 0)
     after = lax.broadcasted_iota(jnp.int32, (tokens, tokens), 1)
-    earlier = jnp.where(before < after, 1.0, 0.0).astype(BF16)
-    rank = dot(hit.astype(BF16), earlier)
-    chosen = jnp.where(rank == turn, hit, 0.0)
-    slot_ref[...] = dot(chosen.astype(BF16), piece).astype(BF16)
-    mix = chosen * weight
+    rank = dot(hit.astype(BF16), jnp.where(before < after, 1.0, 0.0).astype(BF16))
+    return jnp.where(rank == turn, hit, 0.0), same
+
+
+def route_kernel(tp_ref, x_ref, gain_ref, routes_ref, slot_ref, norm_scr, *, side, groups, local_experts, room):
+    norm_scr[...] = normed_rows(x_ref, gain_ref)
+    columns = slot_ref.shape[1]
+    start = pl.multiple_of((lax.rem(tp_ref[0], side) * side + lax.div(tp_ref[0], side)) * columns, columns)
+    chosen, _ = slot_choice(routes_ref, groups, local_experts, room)
+    slot_ref[...] = dot(chosen.astype(BF16), norm_scr[:, pl.ds(start, columns)]).astype(BF16)
+
+
+def route(tp_index, x, gain, routes_t, side, groups, local_experts, room, columns):
+    whole = pl.BlockSpec(memory_space=pltpu.VMEM)
+    return pl.pallas_call(
+        functools.partial(route_kernel, side=side, groups=groups, local_experts=local_experts, room=room),
+        in_specs=[pl.BlockSpec(memory_space=pltpu.SMEM)] + [whole] * 3,
+        out_specs=whole,
+        out_shape=jax.ShapeDtypeStruct((groups * room, columns), BF16),
+        scratch_shapes=[pltpu.VMEM(x.shape, BF16)],
+        name="route",
+    )(tp_index, x, gain, routes_t)
+
+
+def mixture_kernel(
+    x_ref, gain_ref, routes_ref, weight_ref, sg_ref, su_ref, mix_ref, shared_ref, *, groups, local_experts, room
+):
+    chosen, same = slot_choice(routes_ref, groups, local_experts, room)
+    mix = chosen * sum(jnp.where(one, weight_ref[j : j + 1, :], 0.0) for j, one in enumerate(same))
     coarse = mix.astype(BF16)
     mix_ref[0] = coarse
     mix_ref[1] = (mix - coarse.astype(F32)).astype(BF16)
+    normed = normed_rows(x_ref, gain_ref)
     gate_val = dot(normed, sg_ref[...], NT)
     hidden = (gate_val / (1.0 + jnp.exp(-gate_val)) * dot(normed, su_ref[...], NT)).astype(BF16)
     few = shared_ref.shape[0]
-    shared_ref[...] = jnp.concatenate([hidden[n * few : (n + 1) * few] for n in range(tokens // few)], axis=1)
-
-
-def route(tp_index, x, gain, routes_t, weight_t, sg_t, su_t, side, groups, local_experts, room, columns):
-    tokens, width = x.shape
-    slots = groups * room
-    whole = pl.BlockSpec(memory_space=pltpu.VMEM)
-    return pl.pallas_call(
-        functools.partial(route_kernel, side=side, groups=groups, local_experts=local_experts, room=room),
-        in_specs=[pl.BlockSpec(memory_space=pltpu.SMEM)] + [whole] * 6,
-        out_specs=(whole, whole, whole),
+    pieces = [hidden[n * few : (n + 1) * few] for n in range(hidden.shape[0] // few)]
+    shared_ref[...] = jnp.concatenate(pieces, axis=1)
+
+
+def mixture(x, gain, routes_t, weight_t, sg_t, su_t, groups, local_experts, room, columns):
+    tokens = x.shape[0]
+    return pl.pallas_call(
+        functools.partial(mixture_kernel, groups=groups, local_experts=local_experts, room=room),
         out_shape=(
-            jax.ShapeDtypeStruct((slots, columns), BF16),
-            jax.ShapeDtypeStruct((2, slots, tokens), BF16),
+            jax.ShapeDtypeStruct((2, groups * room, tokens), BF16),
             jax.ShapeDtypeStruct((tokens * sg_t.shape[0] // columns, columns), BF16),
         ),
-        scratch_shapes=[pltpu.VMEM((tokens, width), BF16)],
-        name="route",
-    )(tp_index, x, gain, routes_t, weight_t, sg_t, su_t)
+        name="mixture",
+    )(x, gain, routes_t, weight_t, sg_t, su_t)
 
 
 def by_expert(rows, count):
     own = lax.broadcasted_iota(jnp.int32, rows.shape, 0) % count
     return jnp.concatenate([jnp.where(own == e, rows, jnp.zeros((), rows.dtype)) for e in range(count)], axis=1)
+
+
+def compact_kernel(rows_ref, out_ref, scr):
+    sources = rows_ref.shape[0]
+    used = out_ref.shape[1] // sources
+    for n in range(sources):
+        scr[n * used : (n + 1) * used, :] = rows_ref[n].astype(F32)[:used]
+    rows = scr[...].astype(BF16)
+    for n in range(out_ref.shape[0]):
+        out_ref[n] = rows
+
+
+def compact(rows, used, copies):
+    sources, _, columns = rows.shape
+    return pl.pallas_call(
+        compact_kernel,
+        out_shape=jax.ShapeDtypeStruct((copies, sources * used, columns), BF16),
+        scratch_shapes=[pltpu.VMEM((sources * used, columns), F32)],
+        name="compact",
+    )(rows)
 
 
 def partial_kernel(tp_ref, rows_ref, *refs, count, hidden):
@@ -353,32 +381,37 @@
     )(parts, shared)
 
 
-def down_kernel(hidden_ref, w_ref, sw_ref, out_ref, shared_ref, *, side):
+def down_kernel(hidden_ref, w_ref, sw_ref, out_ref, shared_ref, scr, *, side, used):
     count, hidden, columns = w_ref.shape
     peers = hidden_ref.shape[0]
-    each = out_ref.shape[0] // side
+    sources, room, _ = out_ref.shape
+    few = hidden_ref.shape[1] - sources * used // side
+    each = sources * used // side
     w = w_ref[...].reshape(count * hidden, columns)
+    scr[each:, :] = jnp.zeros((scr.shape[0] - each, columns), F32)
     for n in range(side):
         rows = jnp.concatenate([hidden_ref[y * side + n, :each, :] for y in range(side)], axis=1)
-        out_ref[n * each : (n + 1) * each, :] = dot(by_expert(rows, count), w).astype(BF16)
-    few = hidden_ref.shape[1] - each
+        scr[:each, :] = dot(by_expert(rows, count), w)
+        for m in range(sources // side):
+            out_ref[n * (sources // side) + m] = scr[m * used : m * used + room, :].astype(BF16)
     units = sw_ref.shape[0] // peers
     for n in range(shared_ref.shape[0] // few):
         rows = jnp.concatenate([hidden_ref[t, each:, n * units : (n + 1) * units] for t in range(peers)], axis=1)
         shared_ref[n * few : (n + 1) * few, :] = dot(rows, sw_ref[...])
 
 
-def down(hidden, weights, shared_down, side, slots, tokens):
+def down(hidden, weights, shared_down, side, groups, used, room, tokens):
     columns = weights.shape[2]
     whole = pl.BlockSpec(memory_space=pltpu.VMEM)
     return pl.pallas_call(
-        functools.partial(down_kernel, side=side),
+        functools.partial(down_kernel, side=side, used=used),
         in_specs=[whole] * 3,
         out_specs=(whole, whole),
         out_shape=(
-            jax.ShapeDtypeStruct((slots, columns), BF16),
+            jax.ShapeDtypeStruct((groups, room, columns), BF16),
             jax.ShapeDtypeStruct((tokens, columns), F32),
         ),
+        scratch_shapes=[pltpu.VMEM((groups // side * used + 8, columns), F32)],
         name="down",
     )(hidden, weights, shared_down)
 
@@ -423,13 +456,16 @@
     tp_index = lax.axis_index("tp").astype(jnp.int32).reshape(1)
     local_experts, _, hidden_each = expert_gate.shape
     columns = expert_down.shape[2]
-    room = -(-CAP * local_experts // 8) * 8
+    used = CAP * local_experts
+    room = -(-used // 8) * 8
     slot_count = groups * room
     key_value = jnp.concatenate([key_rows.T, value_rows.T], axis=0)
     kv_all = lax.all_gather(key_value, "ep", axis=0)
-    slots, mix, shared = route(
-        tp_index, moe_input, moe_gain.reshape(1, -1), routes.T, route_weight.T, shared_gate.T, shared_up.T,
-        side, groups, local_experts, room, columns,
+    gain = moe_gain.reshape(1, -1)
+    slots = route(tp_index, moe_input, gain, routes.T, side, groups, local_experts, room, columns)
+    mix, shared = mixture(
+        moe_input, gain, routes.T, route_weight.T, shared_gate.T, shared_up.T,
+        groups, local_experts, room, columns,
     )
     arrived = exchanged(slots.reshape(groups, room, columns), "ep")
     pieces = spread_weights(tp_index, expert_gate.transpose(0, 2, 1), expert_up.transpose(0, 2, 1), side)
@@ -437,14 +473,16 @@
     for k in sorted(range(1, side), key=lambda k: -min(k, side - k)):
         steps = [(row[x], row[(x + k) % side]) for row in along_x for x in range(side)]
         pieces[k] = lax.ppermute(pieces[k], "tp", steps)
-    gathered = sent_to_all(arrived.reshape(slot_count, columns), "tp", along_y)
+    gathered = exchanged(compact(arrived, used, side), "tp", along_y)
     parts = partial_products(tp_index, gathered, pieces, local_experts, hidden_each)
     parts = exchanged(parts, "tp", along_x)
     own_hidden = activate(parts, shared, peers)
     hidden = exchanged(own_hidden, "tp")
     state = attention(ep_index, query_rows.T, kv_all, cum_gate, None, own_hidden, peers)
-    result, shared = down(hidden, expert_down, shared_down, side, slot_count, moe_input.shape[0])
-    back = exchanged(result.reshape(groups, room, columns), "ep")
+    result, shared = down(
+        hidden, expert_down, shared_down, side, groups, used, room, moe_input.shape[0]
+    )
+    back = exchanged(result, "ep")
     heads = attention(ep_index, query_rows.T, kv_all, cum_gate, state, result, peers)
     heads = exchanged(heads, "tp")
     mixer_out = projection(heads, out_weight)

time: 242 us -> 238 us (0.983)
  blocking collectives: 46.3 us -> 31 us
  starting transfers between devices: 40.9 us -> 45.9 us
  Pallas kernels: 84.2 us -> 88.2 us
    all_to_all x2 -> x1, blocking collectives: 46.3 us -> 31 us  [exchanged(): lax.all_to_all(array, axis, split_axis=0, concat_axis=0, tiled=True, axis...]
    pallas_call x1 -> x3, Pallas kernels: 3.86 us -> 9.66 us  [the longest x1 3.86 us: mixture(): pl.pallas_call(functools.partial(mixture_kernel, groups=groups, local_exp...]
    all_to_all x4 -> x5, starting transfers between devices: 30.4 us -> 35.4 us  [exchanged(): lax.all_to_all(array, axis, split_axis=0, concat_axis=0, tiled=True, axis...]
    all_to_all x4 -> x5, waiting for transfers between devices: 41 us -> 43.3 us  [exchanged(): lax.all_to_all(array, axis, split_axis=0, concat_axis=0, tiled=True, axis...]
    unnamed x14 -> x16, local copies, waits for them, and re-layouts: 4.28 us -> 5.06 us
  transfers between devices with their start and end apart: 8 -> 9, of which waited for: 4 -> 5; matrix products, arithmetic and copies ran while one was open for 1% -> 0% of each run, Pallas kernels for 34% -> 36%
where the time goes in v4:
time: 238 us; the launch traced here: 237 us
  Pallas kernels  88.2 us (37%)
  waiting for transfers between devices  50.7 us (21%)
  starting transfers between devices  45.9 us (19%)
  blocking collectives  31 us (13%)
  between operations  14.1 us (6%)
  local copies, waits for them, and re-layouts  5.06 us (2%)
    pallas_call x2, Pallas kernels, attention(): pl.pallas_call(functools.partial(attention_kernel, tile=384, opening=open...  61.6 us
    all_to_all x5, waiting for transfers between devices, exchanged(): lax.all_to_all(array, axis, split_axis=0, concat_axis=0, tiled=True, axis...  43.3 us
    all_to_all x5, starting transfers between devices, exchanged(): lax.all_to_all(array, axis, split_axis=0, concat_axis=0, tiled=True, axis...  35.4 us
    all_to_all x1, blocking collectives, exchanged(): lax.all_to_all(array, axis, split_axis=0, concat_axis=0, tiled=True, axis...  31 us
    ppermute x3, starting transfers between devices, local(): pieces[k] = lax.ppermute(pieces[k], 'tp', steps)  10.5 us
    ppermute x3, waiting for transfers between devices, local(): pieces[k] = lax.ppermute(pieces[k], 'tp', steps)  7.43 us
    unnamed x16, local copies, waits for them, and re-layouts  5.06 us
  transfers between devices with their start and end apart: 9, of which 5 were waited for; matrix products, arithmetic and copies ran while one was open for 0% of the time, Pallas kernels for 36%

profile of v4, /device:TPU:481, one launch (start us, length us, event | category | flops | bytes accessed | tf_op | source)
XLA Modules:
  0.0 236.7 jit_solution(592604534739757521)
XLA Ops:
  8.9 3.0 %route.1 = bf16[1280,128]{1,0:T(8,128)(2,1)} custom-call(s32[1]{0:T(128)} %bitcast.5.tp_ref, bf16[192,2048]{1,0:T(8,128)(2,1)} %x_ref.3, f32[1,2048]{1,0:T(1,128)} %bitcast.23, s32[3,192]{1,0:T(4,128)} %bitcast.25), custom_call_target="tpu_custom_call" | custom-call | tf_op jit(solution)/shard_map/route/pallas_call | solution.py:264
  11.9 31.0 %all_to_all.30.rows_ref = bf16[32,40,128]{2,1,0:T(8,128)(2,1)} all-to-all(bf16[32,40,128]{2,1,0:T(8,128)(2,1)} %bitcast.16), channel_id=1, replica_groups=mesh['ep'=32,'tp'=16] {'ep'}, dimensions={0} | all-to-all | bytes 655360 | tf_op jit(solution)/shard_map/all_to_all | solution.py:28
  45.0 4.2 %all-to-all-start.1 = ((bf16[4,1152,128]{2,1,0:T(8,128)(2,1)}), bf16[4,1152,128]{2,1,0:T(8,128)(2,1)S(1)}, u32[]{:S(2)}, u32[]{:S(2)}) async-start(bf16[4,1152,128]{2,1,0:T(8,128)(2,1)} %compact.1), calls=%async_computation.1 | async-start | bytes 2359296 | tf_op jit(solution)/shard_map/all_to_all | solution.py:28
  49.2 2.3 spread.1
  51.5 3.1 %collective-permute-start = (bf16[256,512]{1,0:T(8,128)(2,1)}, bf16[256,512]{1,0:T(8,128)(2,1)S(1)}, u32[]{:S(2)}, u32[]{:S(2)}) collective-permute-start(bf16[256,512]{1,0:T(8,128)(2,1)} %get-tuple-element.13), channel_id=1, source_target_pairs={{0,1},{1,2},{2,3},{3,0},{4,5},{5,6},{6,7},{7,4},{8,9},{9,10},{10,1... | collective-permute-start | bytes 786440 | tf_op jit(solution)/shard_map/ppermute | solution.py:475
  54.6 4.4 %collective-permute-start.1 = (bf16[256,512]{1,0:T(8,128)(2,1)}, bf16[256,512]{1,0:T(8,128)(2,1)S(1)}, u32[]{:S(2)}, u32[]{:S(2)}) collective-permute-start(bf16[256,512]{1,0:T(8,128)(2,1)} %get-tuple-element.14), channel_id=1, source_target_pairs={{0,2},{1,3},{2,0},{3,1},{4,6},{5,7},{6,4},{7,5},{8,10},{9,11},{10,... | collective-permute-start | bytes 786440 | tf_op jit(solution)/shard_map/ppermute | solution.py:475
  59.0 3.1 %collective-permute-start.2 = (bf16[256,512]{1,0:T(8,128)(2,1)}, bf16[256,512]{1,0:T(8,128)(2,1)S(1)}, u32[]{:S(2)}, u32[]{:S(2)}) collective-permute-start(bf16[256,512]{1,0:T(8,128)(2,1)} %get-tuple-element.15), channel_id=1, source_target_pairs={{0,3},{1,0},{2,1},{3,2},{4,7},{5,4},{6,5},{7,6},{8,11},{9,8},{10,9... | collective-permute-start | bytes 786440 | tf_op jit(solution)/shard_map/ppermute | solution.py:475
  62.1 5.3 %collective-permute-done.1.refs_2_ = bf16[256,512]{1,0:T(8,128)(2,1)S(1)} collective-permute-done((bf16[256,512]{1,0:T(8,128)(2,1)}, bf16[256,512]{1,0:T(8,128)(2,1)S(1)}, u32[]{:S(2)}, u32[]{:S(2)}) %collective-permute-start.1) | collective-permute-done | bytes 262176 | tf_op jit(solution)/shard_map/ppermute | solution.py:475
  67.4 2.1 collective-permute-done.2.refs_3_
  70.6 4.0 %partial.1 = bf16[4,288,256]{2,1,0:T(8,128)(2,1)} custom-call(s32[1]{0:T(128)} %bitcast.5.tp_ref, bf16[4,1152,128]{2,1,0:T(8,128)(2,1)} %copy-done.2, bf16[256,512]{1,0:T(8,128)(2,1)} %get-tuple-element.12.refs_0_, bf16[256,512]{1,0:T(8,128)(2,1)} %copy-done.5, bf16[256,512]{1,0:T(8,128)(2,1)} %copy-done.6, bf16[256,512]{1,0:T(8,128)(2,1)} %copy-done.7), custom_call_target="tpu_custom_call" | custom-call | tf_op jit(solution)/shard_map/partial/pallas_call | solution.py:353
  74.6 4.8 %all-to-all-start.2 = ((bf16[4,288,256]{2,1,0:T(8,128)(2,1)}), bf16[4,288,256]{2,1,0:T(8,128)(2,1)S(1)}, u32[]{:S(2)}, u32[]{:S(2)}) async-start(bf16[4,288,256]{2,1,0:T(8,128)(2,1)} %partial.1), calls=%async_computation.2 | async-start | bytes 1179648 | tf_op jit(solution)/shard_map/all_to_all | solution.py:28
  79.4 3.9 %mixture.1 = (bf16[2,1280,192]{2,1,0:T(8,128)(2,1)}, bf16[48,128]{1,0:T(8,128)(2,1)}) custom-call(bf16[192,2048]{1,0:T(8,128)(2,1)} %x_ref.3, f32[1,2048]{1,0:T(1,128)} %bitcast.24, s32[3,192]{1,0:T(4,128)} %bitcast.26, f32[3,192]{1,0:T(4,128)} %bitcast.27, bf16[32,2048]{1,0:T(8,128)(2,1)} %bitcast.19, bf16[32,2048]{1,0:T(8,128)(2,1)} %bitcast.20), custom_call_target="tpu_custom_call" | custom-call | tf_op jit(solution)/shard_map/mixture/pallas_call | solution.py:292
  83.3 4.5 %all-to-all-done.2.parts_ref = bf16[4,288,256]{2,1,0:T(8,128)(2,1)S(1)} async-done(((bf16[4,288,256]{2,1,0:T(8,128)(2,1)}), bf16[4,288,256]{2,1,0:T(8,128)(2,1)S(1)}, u32[]{:S(2)}, u32[]{:S(2)}) %all-to-all-start.2) | async-done | bytes 589856 | tf_op jit(solution)/shard_map/all_to_all | solution.py:28
  88.6 2.3 activate.1.refs_4_
  90.9 6.5 %all-to-all-start.3 = ((bf16[16,336,128]{2,1,0:T(8,128)(2,1)}), bf16[16,336,128]{2,1,0:T(8,128)(2,1)S(1)}, u32[]{:S(2)}, u32[]{:S(2)}) async-start(bf16[16,336,128]{2,1,0:T(8,128)(2,1)} %activate.1.refs_4_), calls=%async_computation.3 | async-start | bytes 2752512 | tf_op jit(solution)/shard_map/all_to_all | solution.py:28
  97.4 18.5 %all-to-all-done.3.hidden_ref = bf16[16,336,128]{2,1,0:T(8,128)(2,1)S(1)} async-done(((bf16[16,336,128]{2,1,0:T(8,128)(2,1)}), bf16[16,336,128]{2,1,0:T(8,128)(2,1)S(1)}, u32[]{:S(2)}, u32[]{:S(2)}) %all-to-all-start.3) | async-done | bytes 1376288 | tf_op jit(solution)/shard_map/all_to_all | solution.py:28
  117.0 3.7 %down.1 = (bf16[32,40,128]{2,1,0:T(8,128)(2,1)}, f32[192,128]{1,0:T(8,128)}) custom-call(bf16[16,336,128]{2,1,0:T(8,128)(2,1)} %copy-done.1, bf16[4,512,128]{2,1,0:T(8,128)(2,1)} %w_ref.2, bf16[512,128]{1,0:T(8,128)(2,1)} %sw_ref.1), custom_call_target="tpu_custom_call" | custom-call | tf_op jit(solution)/shard_map/down/pallas_call | solution.py:406
  120.7 13.6 %all-to-all-start.5 = ((bf16[32,40,128]{2,1,0:T(8,128)(2,1)}), bf16[32,40,128]{2,1,0:T(8,128)(2,1)S(1)}, u32[]{:S(2)}, u32[]{:S(2)}) async-start(bf16[32,40,128]{2,1,0:T(8,128)(2,1)} %get-tuple-element.19.refs_6_), calls=%async_computation.5 | async-start | bytes 655360 | tf_op jit(solution)/shard_map/all_to_all | solution.py:28
  134.4 33.2 %attention_first.1 = (f32[768,128]{1,0:T(8,128)}, f32[768,128]{1,0:T(8,128)}) custom-call(s32[1]{0:T(128)} %bitcast.ep_ref, bf16[64,768]{1,0:T(8,128)(2,1)} %bitcast.30, bf16[32,128,768]{2,1,0:T(8,128)(2,1)} %bitcast.28, f32[1,24576]{1,0:T(1,128)} %refs_3_.3, f32[1,24576]{1,0:T(1,128)} %refs_3_.3, bf16[16,336,128]{2,1,0:T(8,128)(2,1)} %activate.1.refs_4_), custom_call_target="tpu_custom_call" | custom-call | flops 9663676416 | bytes 4194304 | tf_op jit(solution)/shard_map/attention_first/pallas_call | solution.py:155
  167.7 28.4 %attention_rest.1 = bf16[16,384,128]{2,1,0:T(8,128)(2,1)} custom-call(s32[1]{0:T(128)} %bitcast.ep_ref, bf16[64,768]{1,0:T(8,128)(2,1)} %bitcast.31, bf16[32,128,768]{2,1,0:T(8,128)(2,1)} %bitcast.29, f32[1,24576]{1,0:T(1,128)} %refs_3_.3, f32[1,24576]{1,0:T(1,128)} %refs_3_.3, f32[768,128]{1,0:T(8,128)} %get-tuple-element.17.refs_4_, ...), custom_call_target="tpu_custom_call" | custom-call | flops 9663676416 | bytes 4194304 | tf_op jit(solution)/shard_map/attention_rest/pallas_call | solution.py:155
  196.8 6.3 %all-to-all-start.4 = ((bf16[16,384,128]{2,1,0:T(8,128)(2,1)}), bf16[16,384,128]{2,1,0:T(8,128)(2,1)S(1)}, u32[]{:S(2)}, u32[]{:S(2)}) async-start(bf16[16,384,128]{2,1,0:T(8,128)(2,1)} %attention_rest.1), calls=%async_computation.4 | async-start | bytes 3145728 | tf_op jit(solution)/shard_map/all_to_all | solution.py:28
  203.1 2.6 %combine.1 = bf16[192,128]{1,0:T(8,128)(2,1)} custom-call(bf16[2,1280,192]{2,1,0:T(8,128)(2,1)} %get-tuple-element.20.mix_ref, bf16[1280,128]{1,0:T(8,128)(2,1)} %bitcast.15, f32[192,128]{1,0:T(8,128)} %get-tuple-element.21.shared_ref), custom_call_target="tpu_custom_call" | custom-call | tf_op jit(solution)/shard_map/combine/pallas_call | solution.py:426
  205.7 20.3 %all-to-all-done.4.heads_ref = bf16[16,384,128]{2,1,0:T(8,128)(2,1)S(1)} async-done(((bf16[16,384,128]{2,1,0:T(8,128)(2,1)}), bf16[16,384,128]{2,1,0:T(8,128)(2,1)S(1)}, u32[]{:S(2)}, u32[]{:S(2)}) %all-to-all-start.4) | async-done | bytes 1572896 | tf_op jit(solution)/shard_map/all_to_all | solution.py:28
  227.2 2.7 %projection.1 = bf16[768,128]{1,0:T(8,128)(2,1)} custom-call(bf16[16,384,128]{2,1,0:T(8,128)(2,1)} %copy-done, bf16[1024,128]{1,0:T(8,128)(2,1)} %w_ref.3), custom_call_target="tpu_custom_call" | custom-call | flops 402653184 | bytes 4194304 | tf_op jit(solution)/shard_map/projection/pallas_call | solution.py:201
  (24 shorter events, 8.9 us)
Async XLA Ops:
  7.2 127.3 %all-gather.3.cloned.1.call-start = ((), (), s32[]{:S(2)}) async-start(), calls=%async_computation.6 | async-start | bytes 6488064 | tf_op jit(solution)/shard_map/all_gather | solution.py:463
  45.0 24.5 %all-to-all-start.1 = ((bf16[4,1152,128]{2,1,0:T(8,128)(2,1)}), bf16[4,1152,128]{2,1,0:T(8,128)(2,1)S(1)}, u32[]{:S(2)}, u32[]{:S(2)}) async-start(bf16[4,1152,128]{2,1,0:T(8,128)(2,1)} %compact.1), calls=%async_computation.1 | async-start | bytes 2359296 | tf_op jit(solution)/shard_map/all_to_all | solution.py:28
  51.5 10.6 %collective-permute-start = (bf16[256,512]{1,0:T(8,128)(2,1)}, bf16[256,512]{1,0:T(8,128)(2,1)S(1)}, u32[]{:S(2)}, u32[]{:S(2)}) collective-permute-start(bf16[256,512]{1,0:T(8,128)(2,1)} %get-tuple-element.13), channel_id=1, source_target_pairs={{0,1},{1,2},{2,3},{3,0},{4,5},{5,6},{6,7},{7,4},{8,9},{9,10},{10,1... | collective-permute-start | bytes 786440 | tf_op jit(solution)/shard_map/ppermute | solution.py:475
  54.6 12.8 %collective-permute-start.1 = (bf16[256,512]{1,0:T(8,128)(2,1)}, bf16[256,512]{1,0:T(8,128)(2,1)S(1)}, u32[]{:S(2)}, u32[]{:S(2)}) collective-permute-start(bf16[256,512]{1,0:T(8,128)(2,1)} %get-tuple-element.14), channel_id=1, source_target_pairs={{0,2},{1,3},{2,0},{3,1},{4,6},{5,7},{6,4},{7,5},{8,10},{9,11},{10,... | collective-permute-start | bytes 786440 | tf_op jit(solution)/shard_map/ppermute | solution.py:475
  59.0 10.5 %collective-permute-start.2 = (bf16[256,512]{1,0:T(8,128)(2,1)}, bf16[256,512]{1,0:T(8,128)(2,1)S(1)}, u32[]{:S(2)}, u32[]{:S(2)}) collective-permute-start(bf16[256,512]{1,0:T(8,128)(2,1)} %get-tuple-element.15), channel_id=1, source_target_pairs={{0,3},{1,0},{2,1},{3,2},{4,7},{5,4},{6,5},{7,6},{8,11},{9,8},{10,9... | collective-permute-start | bytes 786440 | tf_op jit(solution)/shard_map/ppermute | solution.py:475
  62.1 7.5 %copy-start.5 = (bf16[256,512]{1,0:T(8,128)(2,1)}, bf16[256,512]{1,0:T(8,128)(2,1)S(1)}, u32[]{:S(2)}) copy-start(bf16[256,512]{1,0:T(8,128)(2,1)S(1)} %collective-permute-done.refs_1_) | copy-start | bytes 786436
  67.4 2.1 copy-start.6
  69.5 0.7 copy-start.7
  69.5 1.1 copy-start.2
  74.6 13.1 %all-to-all-start.2 = ((bf16[4,288,256]{2,1,0:T(8,128)(2,1)}), bf16[4,288,256]{2,1,0:T(8,128)(2,1)S(1)}, u32[]{:S(2)}, u32[]{:S(2)}) async-start(bf16[4,288,256]{2,1,0:T(8,128)(2,1)} %partial.1), calls=%async_computation.2 | async-start | bytes 1179648 | tf_op jit(solution)/shard_map/all_to_all | solution.py:28
  87.7 0.9 copy-start.3
  90.9 25.0 %all-to-all-start.3 = ((bf16[16,336,128]{2,1,0:T(8,128)(2,1)}), bf16[16,336,128]{2,1,0:T(8,128)(2,1)S(1)}, u32[]{:S(2)}, u32[]{:S(2)}) async-start(bf16[16,336,128]{2,1,0:T(8,128)(2,1)} %activate.1.refs_4_), calls=%async_computation.3 | async-start | bytes 2752512 | tf_op jit(solution)/shard_map/all_to_all | solution.py:28
  115.8 1.2 copy-start.1
  120.7 75.3 %all-to-all-start.5 = ((bf16[32,40,128]{2,1,0:T(8,128)(2,1)}), bf16[32,40,128]{2,1,0:T(8,128)(2,1)S(1)}, u32[]{:S(2)}, u32[]{:S(2)}) async-start(bf16[32,40,128]{2,1,0:T(8,128)(2,1)} %get-tuple-element.19.refs_6_), calls=%async_computation.5 | async-start | bytes 655360 | tf_op jit(solution)/shard_map/all_to_all | solution.py:28
  196.0 0.8 copy-start.4
  196.8 29.2 %all-to-all-start.4 = ((bf16[16,384,128]{2,1,0:T(8,128)(2,1)}), bf16[16,384,128]{2,1,0:T(8,128)(2,1)S(1)}, u32[]{:S(2)}, u32[]{:S(2)}) async-start(bf16[16,384,128]{2,1,0:T(8,128)(2,1)} %attention_rest.1), calls=%async_computation.4 | async-start | bytes 3145728 | tf_op jit(solution)/shard_map/all_to_all | solution.py:28
  226.0 1.2 copy-start
Sparse Core Ops, SparseCore 0:
  10.7 81.9 all-gather.2
